TPU v7x, 128 devices: a whole 4x4x4 slice. The times are simulated.
128 devices in a mesh: kv: 16 (over z, y), tp: 8 (over x, core).
Axes of the slice: x: 4, y: 4, z: 4, core: 2. Of those that a mesh axis runs over, the one named last changes fastest.
Arguments:
- tokens: bfloat16 [32, 4096], P(None, ('kv', 'tp')), may hold values from -36 to 36
- first_gain: float32 [4096], P('kv'), may hold values from 0.1 to 1.9
- first_gate: bfloat16 [4096, 11264], P('kv', 'tp'), may hold values from -0.09375 to 0.09375
- first_up: bfloat16 [4096, 11264], P('kv', 'tp'), may hold values from -0.09375 to 0.09375
- first_down: bfloat16 [11264, 4096], P('tp', 'kv'), may hold values from -0.0546875 to 0.0546875
- mix_gain: float32 [4096], P('kv'), may hold values from 0.1 to 1.9
- w_query: bfloat16 [4096, 2048], P('kv', 'tp'), may hold values from -0.09375 to 0.09375
- key_cache: bfloat16 [32, 16384, 1024], P(None, 'kv', 'tp'), may hold values from -100 to 100
- value_cache: bfloat16 [32, 16384, 1024], P(None, 'kv', 'tp'), may hold values from -6 to 6
- map_weight: float32 [32], P('tp'), may hold values from 0.3 to 0.8
- head_gain: float32 [64], replicated, may hold values from 0.1 to 1.9
- w_out: bfloat16 [2048, 4096], P('tp', 'kv'), may hold values from -0.125 to 0.125
- second_gain: float32 [4096], P('kv'), may hold values from 0.1 to 1.9
- second_gate: bfloat16 [4096, 11264], P('kv', 'tp'), may hold values from -0.09375 to 0.09375
- second_up: bfloat16 [4096, 11264], P('kv', 'tp'), may hold values from -0.09375 to 0.09375
- second_down: bfloat16 [11264, 4096], P('tp', 'kv'), may hold values from -0.0546875 to 0.0546875
Outputs:
- mixed: bfloat16 [32, 4096], P(None, ('kv', 'tp'))
All inputs are finite; a program needn't handle non-finite values.
Results may differ from a plain program's by a relative error of at most 0.0158.
Values may be sent and summed in bfloat16 or wider, within the bound.
A program may use at most 128 MiB of HBM per device.

v0:
```python
import functools
import math

import jax
import jax.numpy as jnp
from jax import lax
from jax.experimental import pallas as pl
from jax.experimental.pallas import tpu as pltpu
from jax.sharding import PartitionSpec as P

HEAD = 64
MAPS = 2
LANES = 128
TILE = 8
EPS = 1e-06
HEAD_SCALE = 0.8
F32 = jnp.float32
BF16 = jnp.bfloat16
MESH = pl.DeviceIdType.MESH
VMEM_LIMIT = 60 * 1024 * 1024


def greet(axes):
    barrier = pltpu.get_barrier_semaphore()
    total = 0
    for axis, n in axes:
        me = lax.axis_index(axis)
        for k in range(1, n):
            pl.semaphore_signal(
                barrier, inc=1, device_id={axis: lax.rem(me + k, n)}, device_id_type=MESH
            )
        total += n - 1
    pl.semaphore_wait(barrier, total)


def exchange(axis, n, source, target, sems):
    me = lax.axis_index(axis)
    copies = []
    for k in range(1, n):
        dest = lax.rem(me + k, n)
        copy = pltpu.make_async_remote_copy(
            src_ref=source(dest),
            dst_ref=target(k - 1),
            send_sem=sems.at[0, k - 1],
            recv_sem=sems.at[1, k - 1],
            device_id={axis: dest},
            device_id_type=MESH,
        )
        copy.start()
        copies.append(copy)
    return copies


def total_of(copies, own, recv):
    total = own
    for k, copy in enumerate(copies):
        copy.wait()
        total = total + recv[k].astype(F32)
    return total


def squares_tile(h):
    s = jnp.sum(h * h, axis=1, keepdims=True)
    high = s.astype(BF16).astype(F32)
    lane = lax.broadcasted_iota(jnp.int32, (h.shape[0], LANES), 1)
    return jnp.where(lane < LANES // 2, high, s - high).astype(BF16)


def row_factor(tile, width):
    s = tile[:, :1] + tile[:, LANES // 2 : LANES // 2 + 1]
    return lax.rsqrt(s / width + EPS)


def chunk_width(hidden, n):
    return -(-hidden // (LANES * n)) * LANES


def dot(a, b):
    return jnp.dot(a, b, preferred_element_type=F32)


def feed_forward(n_kv, h, gain, w_gate, w_up, w_down, loads, scratch):
    send, recv, act_own, act_all, rs_sems, ag_sems = scratch
    me = lax.axis_index("kv")
    hidden = w_gate.shape[1]
    cw = chunk_width(hidden, n_kv)
    rows = h.shape[0]
    tile = squares_tile(h)
    scaled = (h * gain).astype(BF16)
    loads[0].wait()
    loads[1].wait()
    for j in range(n_kv):
        low = min(j * cw, hidden)
        w = min(cw, hidden - low)
        for base, weight in ((0, w_gate), (cw, w_up)):
            if w > 0:
                send[j, :, base : base + w] = dot(scaled, weight[:, low : low + w]).astype(BF16)
            if w < cw:
                send[j, :, base + w : base + cw] = jnp.zeros((rows, cw - w), BF16)
        send[j, :, 2 * cw :] = tile
    copies = exchange("kv", n_kv, lambda d: send.at[d], lambda k: recv.at[k], rs_sems)
    total = total_of(copies, send[me].astype(F32), recv)
    factor = row_factor(total[:, 2 * cw :], h.shape[1] * n_kv)
    gate = total[:, :cw] * factor
    up = total[:, cw : 2 * cw] * factor
    act = (gate / (1.0 + jnp.exp(-gate)) * up).astype(BF16)
    act_own[...] = act
    mine = pl.ds(pl.multiple_of(me * cw, LANES), cw)
    act_all[:, mine] = act
    copies = exchange("kv", n_kv, lambda d: act_own, lambda k: act_all.at[:, mine], ag_sems)
    for copy in copies:
        copy.wait()
    loads[2].wait()
    return dot(act_all[:, :hidden], w_down[...])


def sum_over_tp(n_tp, part, send, recv, sems):
    send[...] = part.astype(BF16)
    copies = exchange("tp", n_tp, lambda d: send, lambda k: recv.at[k], sems)
    return total_of(copies, send[...].astype(F32), recv)


def start_loads(pairs, sems):
    loads = [pltpu.make_async_copy(a, b, sems.at[i]) for i, (a, b) in enumerate(pairs)]
    for load in loads:
        load.start()
    return loads


def first_kernel(
    n_kv, n_tp, tokens, gain, mix_gain, gate_any, up_any, down_any, query_any, h_out, q_out,
    w_gate, w_up, w_down, w_query, tok_all, rs_send, rs_recv, act_own, act_all,
    tp_send, tp_recv, q_send, q_recv, load_sems, tok_sems, rs_sems, ag_sems, tp_sems, q_sems,
):
    loads = start_loads(
        ((gate_any, w_gate), (up_any, w_up), (down_any, w_down), (query_any, w_query)), load_sems
    )
    greet((("kv", n_kv), ("tp", n_tp)))
    tp = lax.axis_index("tp")
    tok_all[tp] = tokens[...]
    copies = exchange("tp", n_tp, lambda d: tokens, lambda k: tok_all.at[tp], tok_sems)
    for copy in copies:
        copy.wait()
    h = jnp.concatenate([tok_all[j].astype(F32) for j in range(n_tp)], axis=1)
    part = feed_forward(
        n_kv, h, gain[...], w_gate, w_up, w_down, loads,
        (rs_send, rs_recv, act_own, act_all, rs_sems, ag_sems),
    )
    h = h + 0.5 * sum_over_tp(n_tp, part, tp_send, tp_recv, tp_sems)
    h_out[...] = h
    loads[3].wait()
    columns = w_query.shape[1]
    q_send[:, :columns] = dot((h * mix_gain[...]).astype(BF16), w_query[...]).astype(BF16)
    q_send[:, columns:] = squares_tile(h)
    copies = exchange("kv", n_kv, lambda d: q_send, lambda k: q_recv.at[k], q_sems)
    total = total_of(copies, q_send[...].astype(F32), q_recv)
    factor = row_factor(total[:, columns:], h.shape[1] * n_kv)
    q_out[...] = (total[:, :columns] * factor).astype(BF16)


def attention_kernel(kv_local, per_tile, scale, q_ref, k_ref, v_ref, o_ref, lse_ref):
    wide = lax.broadcasted_iota(jnp.int32, (TILE, kv_local * HEAD), 1) // HEAD
    lane = lax.broadcasted_iota(jnp.int32, (TILE, LANES), 1)
    part_rows = TILE // per_tile
    wide_row = lax.broadcasted_iota(jnp.int32, (TILE, kv_local * HEAD), 0) // part_rows
    lane_row = lax.broadcasted_iota(jnp.int32, (TILE, LANES), 0) // part_rows
    tiles_o, tiles_lse = [], []
    for first in range(0, q_ref.shape[0], per_tile):
        tile_o = jnp.zeros((TILE, kv_local * HEAD), F32)
        tile_lse = jnp.zeros((TILE, LANES), F32)
        for i in range(per_tile):
            b = first + i
            s = scale * lax.dot_general(
                q_ref[b], k_ref[b], (((1,), (1,)), ((), ())), preferred_element_type=F32
            )
            peak = jnp.max(s, axis=1, keepdims=True)
            e = jnp.exp(s - peak)
            l = jnp.sum(e, axis=1, keepdims=True)
            o = dot(e.astype(BF16), v_ref[b]) / l
            lse = peak + jnp.log(l)
            for k in range(kv_local):
                rows = slice(k * TILE, (k + 1) * TILE)
                tile_o = jnp.where((wide == k) & (wide_row == i), o[rows], tile_o)
                tile_lse = jnp.where((lane == k) & (lane_row == i), lse[rows], tile_lse)
        tiles_o.append(tile_o)
        tiles_lse.append(tile_lse)
    o_ref[0] = jnp.concatenate(tiles_o, axis=0).astype(BF16)
    lse_ref[0] = jnp.concatenate(tiles_lse, axis=0)


def second_kernel(
    n_kv, n_tp, kv_local, group, h_in, o_part, lse_part, map_weight, head_gain, gain,
    out_any, gate_any, up_any, down_any, mixed,
    w_out, w_gate, w_up, w_down, o_recv, lse_recv, head_own, head_all, rs_send, rs_recv,
    act_own, act_all, tp_send, tp_recv, fin_send, fin_recv,
    load_sems, o_sems, lse_sems, head_sems, rs_sems, ag_sems, tp_sems, fin_sems,
):
    loads = start_loads(
        ((out_any, w_out), (gate_any, w_gate), (up_any, w_up), (down_any, w_down)), load_sems
    )
    greet((("kv", n_kv), ("tp", n_tp)))
    me = lax.axis_index("kv")
    copies = exchange("kv", n_kv, lambda d: o_part.at[d], lambda k: o_recv.at[k], o_sems)
    copies += exchange("kv", n_kv, lambda d: lse_part.at[d], lambda k: lse_recv.at[k], lse_sems)
    for copy in copies:
        copy.wait()
    lses = [lse_part[me]] + [lse_recv[k] for k in range(n_kv - 1)]
    outs = [o_part[me].astype(F32)] + [o_recv[k].astype(F32) for k in range(n_kv - 1)]
    peak = functools.reduce(jnp.maximum, lses)
    weights = [jnp.exp(lse - peak) for lse in lses]
    scale = 1.0 / functools.reduce(jnp.add, weights)
    slab = outs[0].shape
    head_of = lax.broadcasted_iota(jnp.int32, slab, 1) // HEAD

    def widen(value):
        wide = jnp.zeros(slab, F32)
        for k in range(kv_local):
            wide = jnp.where(head_of == k, value[:, k : k + 1], wide)
        return wide

    merged = functools.reduce(
        jnp.add, [widen(weight * scale) * out for weight, out in zip(weights, outs)]
    )
    diff = merged - map_weight[...] * pltpu.roll(merged, slab[0] - group, 0)
    square = diff * diff
    mean = jnp.zeros(slab, F32)
    for k in range(kv_local):
        here = jnp.sum(jnp.where(head_of == k, square, 0.0), axis=1, keepdims=True) / HEAD
        mean = jnp.where(head_of == k, here, mean)
    head_own[...] = (diff * lax.rsqrt(mean + EPS) * head_gain[...] * HEAD_SCALE).astype(BF16)
    head_all[me] = head_own[...]
    copies = exchange("kv", n_kv, lambda d: head_own, lambda k: head_all.at[me], head_sems)
    for copy in copies:
        copy.wait()
    heads = head_all[...].reshape(n_kv * slab[0], slab[1])
    loads[0].wait()
    batch = h_in.shape[0]
    pick_row = lax.broadcasted_iota(jnp.int32, (batch, heads.shape[0]), 0)
    pick_col = lax.broadcasted_iota(jnp.int32, (batch, heads.shape[0]), 1)
    part = None
    for g in range(group):
        pick = jnp.where(pick_col == pick_row * (MAPS * group) + g, 1.0, 0.0).astype(BF16)
        picked = dot(pick, heads).astype(BF16)
        weight = jnp.concatenate(
            [w_out[(k * group + g) * HEAD : (k * group + g + 1) * HEAD, :] for k in range(kv_local)],
            axis=0,
        )
        term = dot(picked, weight)
        part = term if part is None else part + term
    h = h_in[...] + sum_over_tp(n_tp, part, tp_send, tp_recv, tp_sems)
    part = feed_forward(
        n_kv, h, gain[...], w_gate, w_up, w_down, loads[1:],
        (rs_send, rs_recv, act_own, act_all, rs_sems, ag_sems),
    )
    width = mixed.shape[1]
    tp = lax.axis_index("tp")
    mine = jnp.zeros((batch, width), F32)
    for j in range(n_tp):
        columns = slice(j * width, (j + 1) * width)
        fin_send[j] = part[:, columns].astype(BF16)
        mine = jnp.where(tp == j, h[:, columns], mine)
    copies = exchange("tp", n_tp, lambda d: fin_send.at[d], lambda k: fin_recv.at[k], fin_sems)
    total = total_of(copies, fin_send[tp].astype(F32), fin_recv)
    mixed[...] = (mine + 0.5 * total).astype(BF16)


def dma_sems(n):
    return pltpu.SemaphoreType.DMA((2, n - 1))


def on_device(
    n_kv, n_tp, tokens, first_gain, first_gate, first_up, first_down, mix_gain, w_query,
    key_cache, value_cache, map_weight, head_gain, w_out, second_gain, second_gate, second_up,
    second_down,
):
    batch = tokens.shape[0]
    depth, hidden = first_gate.shape
    length = key_cache.shape[1]
    columns = w_query.shape[1]
    kv_local = key_cache.shape[2] // HEAD
    group = columns // (kv_local * HEAD)
    cw = chunk_width(hidden, n_kv)
    vmem = pl.BlockSpec(memory_space=pltpu.VMEM)
    hbm = pl.BlockSpec(memory_space=pl.ANY)
    ffn_buffers = [
        pltpu.VMEM((n_kv, batch, 2 * cw + LANES), BF16),
        pltpu.VMEM((n_kv - 1, batch, 2 * cw + LANES), BF16),
        pltpu.VMEM((batch, cw), BF16),
        pltpu.VMEM((batch, n_kv * cw), BF16),
    ]
    tp_buffers = [pltpu.VMEM((batch, depth), BF16), pltpu.VMEM((n_tp - 1, batch, depth), BF16)]

    def params(number):
        return pltpu.CompilerParams(
            collective_id=number, has_side_effects=True, vmem_limit_bytes=VMEM_LIMIT
        )

    h1, queries = pl.pallas_call(
        functools.partial(first_kernel, n_kv, n_tp),
        out_shape=(
            jax.ShapeDtypeStruct((batch, depth), F32),
            jax.ShapeDtypeStruct((batch, columns), BF16),
        ),
        in_specs=[vmem] * 3 + [hbm] * 4,
        out_specs=(vmem, vmem),
        scratch_shapes=[
            pltpu.VMEM(first_gate.shape, BF16),
            pltpu.VMEM(first_up.shape, BF16),
            pltpu.VMEM(first_down.shape, BF16),
            pltpu.VMEM(w_query.shape, BF16),
            pltpu.VMEM((n_tp,) + tokens.shape, BF16),
            *ffn_buffers,
            *tp_buffers,
            pltpu.VMEM((batch, columns + LANES), BF16),
            pltpu.VMEM((n_kv - 1, batch, columns + LANES), BF16),
            pltpu.SemaphoreType.DMA((4,)),
            dma_sems(n_tp),
            dma_sems(n_kv),
            dma_sems(n_kv),
            dma_sems(n_tp),
            dma_sems(n_kv),
        ],
        compiler_params=params(1),
    )(
        tokens, first_gain.reshape(1, -1), mix_gain.reshape(1, -1),
        first_gate, first_up, first_down, w_query,
    )

    per_tile = TILE // (MAPS * group)
    q = queries.reshape(batch, kv_local, 1, group, HEAD)
    half = (jnp.arange(HEAD) // (HEAD // MAPS))[None, :] == jnp.arange(MAPS)[:, None]
    q = jnp.where(half[None, None, :, None, :], q, 0).reshape(batch, kv_local, 1, MAPS * group, 1, HEAD)
    place = (jnp.arange(batch) % per_tile)[:, None] == jnp.arange(per_tile)[None, :]
    own = jnp.arange(kv_local)[:, None] == jnp.arange(kv_local)[None, :]
    keep = place[:, None, :, None, None, None] & own[None, :, None, None, :, None]
    q = jnp.where(keep, q, 0).reshape(batch, kv_local * TILE, kv_local * HEAD)

    each = batch // n_kv
    slab_rows = each // per_tile * TILE
    o_part, lse_part = pl.pallas_call(
        functools.partial(attention_kernel, kv_local, per_tile, 1.0 / math.sqrt(HEAD // MAPS)),
        grid=(n_kv,),
        out_shape=(
            jax.ShapeDtypeStruct((n_kv, slab_rows, kv_local * HEAD), BF16),
            jax.ShapeDtypeStruct((n_kv, slab_rows, LANES), F32),
        ),
        in_specs=[
            pl.BlockSpec((each, kv_local * TILE, kv_local * HEAD), lambda i: (i, 0, 0)),
            pl.BlockSpec((each, length, kv_local * HEAD), lambda i: (i, 0, 0)),
            pl.BlockSpec((each, length, kv_local * HEAD), lambda i: (i, 0, 0)),
        ],
        out_specs=(
            pl.BlockSpec((1, slab_rows, kv_local * HEAD), lambda i: (i, 0, 0)),
            pl.BlockSpec((1, slab_rows, LANES), lambda i: (i, 0, 0)),
        ),
        compiler_params=pltpu.CompilerParams(vmem_limit_bytes=VMEM_LIMIT),
    )(q, key_cache, value_cache)

    weight = jnp.repeat(map_weight.reshape(kv_local, group).T, HEAD, axis=1)
    weight = jnp.tile(weight, (slab_rows // group, 1))
    gain = jnp.tile(head_gain, kv_local).reshape(1, -1)
    width = depth // n_tp
    return pl.pallas_call(
        functools.partial(second_kernel, n_kv, n_tp, kv_local, group),
        out_shape=jax.ShapeDtypeStruct((batch, width), BF16),
        in_specs=[vmem] * 6 + [hbm] * 4,
        out_specs=vmem,
        scratch_shapes=[
            pltpu.VMEM(w_out.shape, BF16),
            pltpu.VMEM(second_gate.shape, BF16),
            pltpu.VMEM(second_up.shape, BF16),
            pltpu.VMEM(second_down.shape, BF16),
            pltpu.VMEM((n_kv - 1,) + o_part.shape[1:], BF16),
            pltpu.VMEM((n_kv - 1,) + lse_part.shape[1:], F32),
            pltpu.VMEM(o_part.shape[1:], BF16),
            pltpu.VMEM(o_part.shape, BF16),
            *ffn_buffers,
            *tp_buffers,
            pltpu.VMEM((n_tp, batch, width), BF16),
            pltpu.VMEM((n_tp - 1, batch, width), BF16),
            pltpu.SemaphoreType.DMA((4,)),
            dma_sems(n_kv),
            dma_sems(n_kv),
            dma_sems(n_kv),
            dma_sems(n_kv),
            dma_sems(n_kv),
            dma_sems(n_tp),
            dma_sems(n_tp),
        ],
        compiler_params=params(2),
    )(
        h1, o_part, lse_part, weight, gain, second_gain.reshape(1, -1),
        w_out, second_gate, second_up, second_down,
    )


def solution(mesh):
    placed = (
        P(None, ("kv", "tp")),
        P("kv"),
        P("kv", "tp"),
        P("kv", "tp"),
        P("tp", "kv"),
        P("kv"),
        P("kv", "tp"),
        P(None, "kv", "tp"),
        P(None, "kv", "tp"),
        P("tp"),
        P(),
        P("tp", "kv"),
        P("kv"),
        P("kv", "tp"),
        P("kv", "tp"),
        P("tp", "kv"),
    )
    return jax.shard_map(
        functools.partial(on_device, mesh.shape["kv"], mesh.shape["tp"]),
        mesh=mesh,
        in_specs=placed,
        out_specs=P(None, ("kv", "tp")),
        check_vma=False,
    )
```

profile of v0, /device:TPU:1, one launch (start us, length us, event | category | flops | bytes accessed | tf_op | source)
XLA Modules:
  0.0 100.1 jit_solution(12769925489674685906)
XLA Ops:
  0.0 38.7 %shard_map.154 = (f32[32,256]{1,0:T(8,128)}, bf16[32,256]{1,0:T(8,128)(2,1)}) custom-call(bf16[32,32]{1,0:T(8,128)(2,1)} %tokens.1, f32[1,256]{1,0:T(1,128)} %bitcast.9, f32[1,256]{1,0:T(1,128)} %bitcast.10, bf16[256,1408]{1,0:T(8,128)(2,1)} %gate_any.2, bf16[256,1408]{1,0:T(8,128)(2,1)} %up_any.2, bf16[1408,256]{1,0:T(8,128)(2,1)} %down_any.2, ...), custom_call_target="tpu_custom_call" | custom-call | tf_op jit(solution)/shard_map/pallas_call | solution.py:298
  38.7 0.1 iota_compare_fusion
  38.8 0.1 broadcast_and_fusion
  38.9 0.8 broadcast_in_dim.64
  39.8 0.3 broadcast_select_fusion
  40.2 0.8 select_n.40.q_ref
  41.0 0.0 copy-start
  41.0 0.0 copy-start.1
  41.0 17.3 %shard_map.155 = (bf16[16,8,128]{2,1,0:T(8,128)(2,1)}, f32[16,8,128]{2,1,0:T(8,128)}) custom-call(bf16[32,16,128]{2,1,0:T(8,128)(2,1)} %select_n.40.q_ref, bf16[32,1024,128]{2,1,0:T(8,128)(2,1)} %k_ref.1, bf16[32,1024,128]{2,1,0:T(8,128)(2,1)} %v_ref.1), custom_call_target="tpu_custom_call" | custom-call | tf_op jit(solution)/shard_map/pallas_call | solution.py:340
  58.3 0.0 copy-done
  58.3 0.1 reshape.116
  58.3 0.1 copy.17
  58.4 0.1 broadcast_in_dim.70
  58.5 0.1 tile.16
  58.6 0.6 tile.17
  59.2 0.0 copy-done.1
  59.2 0.6 reshape_tile.3.head_gain
  59.8 39.0 %shard_map.156 = bf16[32,32]{1,0:T(8,128)(2,1)} custom-call(f32[32,256]{1,0:T(8,128)} %get-tuple-element.9.h_in, bf16[16,8,128]{2,1,0:T(8,128)(2,1)} %get-tuple-element.11.o_part, f32[16,8,128]{2,1,0:T(8,128)} %get-tuple-element.12.lse_part, f32[8,128]{1,0:T(8,128)} %bitcast.7, f32[1,128]{1,0:T(1,128)} %reshape_tile.3.head_gain, f32[1,256]{1,0:T(1,128)} %bitcast.8, ...), custom_call_target="tpu_custom_call" | custom-call | tf_op jit(solution)/shard_map/pallas_call | solution.py:363
  98.8 1.3 %copy.19 = bf16[32,32]{1,0:T(8,128)(2,1)} copy(bf16[32,32]{1,0:T(8,128)(2,1)} %shard_map.156) | data formatting | bytes 4096
  (9 shorter events, 0.1 us)
Async XLA Ops:
  41.0 17.3 %copy-start = (f32[4]{0:T(128)S(1)}, f32[4]{0:T(128)}, u32[]{:S(2)}) copy-start(f32[4]{0:T(128)} %param.25) | copy-start | bytes 52
  41.0 18.2 %copy-start.1 = (f32[64]{0:T(128)S(1)}, f32[64]{0:T(128)}, u32[]{:S(2)}) copy-start(f32[64]{0:T(128)} %param.26) | copy-start | bytes 772
where the time goes:
time: 101 us; the launch traced here: 100 us
  Pallas kernels  94.9 us (94%)
  local copies, waits for them, and re-layouts  4.51 us (4%)
    pallas_call x1, Pallas kernels, on_device(): pl.pallas_call(functools.partial(second_kernel, n_kv, n_tp, kv_local, gro...  39 us
    pallas_call x1, Pallas kernels, on_device(): pl.pallas_call(functools.partial(first_kernel, n_kv, n_tp), out_shape=(ja...  38.7 us
    pallas_call x1, Pallas kernels, on_device(): pl.pallas_call(functools.partial(attention_kernel, kv_local, per_tile, 1....  17.3 us

commit v1 on v0

v1 whole, which is shorter than its diff:
```python
import functools
import math

import jax
import jax.numpy as jnp
from jax import lax
from jax.experimental import pallas as pl
from jax.experimental.pallas import tpu as pltpu
from jax.sharding import PartitionSpec as P

HEAD = 64
MAPS = 2
LANES = 128
TILE = 8
EPS = 1e-06
HEAD_SCALE = 0.8
SIDE = 4
ROW_GROUPS = 4
COL_GROUPS = 4
F32 = jnp.float32
BF16 = jnp.bfloat16
MESH = pl.DeviceIdType.MESH
VMEM_LIMIT = 60 * 1024 * 1024


def hops(d):
    return min(d, SIDE - d)


def kv_offsets():
    offs = [(a, b) for a in range(SIDE) for b in range(SIDE) if (a, b) != (0, 0)]
    return sorted(offs, key=lambda o: -(hops(o[0]) + hops(o[1])))


def tp_offsets():
    offs = [(a, b) for a in range(SIDE) for b in range(2) if (a, b) != (0, 0)]
    return sorted(offs, key=lambda o: -(2 * hops(o[0]) + o[1]))


def shifted(axis, offset):
    me = lax.axis_index(axis)
    inner = SIDE if axis == "kv" else 2
    high = lax.rem(me // inner + offset[0], SIDE)
    low = lax.rem(lax.rem(me, inner) + offset[1], inner)
    return high * inner + low


OFFSETS = {"kv": kv_offsets(), "tp": tp_offsets()}


def greet():
    barrier = pltpu.get_barrier_semaphore()
    total = 0
    for axis in ("kv", "tp"):
        for offset in OFFSETS[axis]:
            pl.semaphore_signal(
                barrier, inc=1, device_id={axis: shifted(axis, offset)}, device_id_type=MESH
            )
            total += 1
    pl.semaphore_wait(barrier, total)


def exchange(axis, source, target, sems):
    copies = []
    for k, offset in enumerate(OFFSETS[axis]):
        dest = shifted(axis, offset)
        copy = pltpu.make_async_remote_copy(
            src_ref=source(dest),
            dst_ref=target(k),
            send_sem=sems.at[0, k],
            recv_sem=sems.at[1, k],
            device_id={axis: dest},
            device_id_type=MESH,
        )
        copy.start()
        copies.append(copy)
    return copies


def total_of(copies, own, recv):
    total = own
    for k in reversed(range(len(copies))):
        copies[k].wait()
        total = total + recv[k].astype(F32)
    return total


def dot(a, b):
    return jnp.dot(a, b, preferred_element_type=F32)


def row_squares(h):
    return jnp.sum(h * h, axis=1, keepdims=True)


def squares_tile(h):
    s = row_squares(h)
    high = s.astype(BF16).astype(F32)
    lane = lax.broadcasted_iota(jnp.int32, (h.shape[0], LANES), 1)
    return jnp.where(lane < LANES // 2, high, s - high).astype(BF16)


def row_factor(tile, width):
    s = tile[:, :1] + tile[:, LANES // 2 : LANES // 2 + 1]
    return lax.rsqrt(s / width + EPS)


def feed_forward(n_kv, h, gain, w_gate, w_up, w_down, loads, scratch):
    send, recv, act_own, act_all, rs_sems, ag_sems = scratch
    me = lax.axis_index("kv")
    hidden = w_gate.shape[1]
    cw = act_own.shape[1]
    tile = squares_tile(h)
    scaled = (h * gain).astype(BF16)
    loads[0].wait()
    loads[1].wait()
    for c in range(COL_GROUPS):
        low = c * cw
        w = min(cw, hidden - low)
        for base, weight in ((0, w_gate), (cw, w_up)):
            part = dot(scaled, weight[:, low : low + w])
            for r in range(ROW_GROUPS):
                rows = slice(r * TILE, (r + 1) * TILE)
                send[r * COL_GROUPS + c, :, base : base + w] = part[rows].astype(BF16)
                if w < cw:
                    send[r * COL_GROUPS + c, :, base + w : base + cw] = jnp.zeros(
                        (TILE, cw - w), BF16
                    )
        for r in range(ROW_GROUPS):
            send[r * COL_GROUPS + c, :, 2 * cw :] = tile[r * TILE : (r + 1) * TILE]
    copies = exchange("kv", lambda d: send.at[d], lambda k: recv.at[k], rs_sems)
    total = total_of(copies, send[me].astype(F32), recv)
    factor = row_factor(total[:, 2 * cw :], h.shape[1] * n_kv)
    gate = total[:, :cw] * factor
    up = total[:, cw : 2 * cw] * factor
    act = (gate / (1.0 + jnp.exp(-gate)) * up).astype(BF16)
    act_own[...] = act
    act_all[me] = act
    copies = exchange("kv", lambda d: act_own, lambda k: act_all.at[me], ag_sems)
    for copy in copies:
        copy.wait()
    loads[2].wait()
    out = None
    for c in range(COL_GROUPS):
        low = c * cw
        w = min(cw, hidden - low)
        block = jnp.concatenate(
            [act_all[r * COL_GROUPS + c, :, :w].astype(F32) for r in range(ROW_GROUPS)], axis=0
        ).astype(BF16)
        term = dot(block, w_down[low : low + w, :])
        out = term if out is None else out + term
    return out


def sum_over_tp(part, send, recv, sems):
    send[...] = part.astype(BF16)
    copies = exchange("tp", lambda d: send, lambda k: recv.at[k], sems)
    return total_of(copies, send[...].astype(F32), recv)


def query_step(n_kv, h, gain, w_query, q_send, q_recv, q_sems):
    rows = h.shape[0]
    product = dot((h * gain).astype(BF16), w_query[...])
    row = lax.broadcasted_iota(jnp.int32, (rows, LANES), 0)
    lane = lax.broadcasted_iota(jnp.int32, (rows, LANES), 1)
    s = jnp.sum(jnp.where(row == lane, row_squares(h), 0.0), axis=0, keepdims=True)
    high = s.astype(BF16).astype(F32)
    first = lax.broadcasted_iota(jnp.int32, (TILE, LANES), 0)
    stats = jnp.where(first == 0, high, jnp.where(first == 1, s - high, 0.0))
    tiles = rows // TILE
    for r in range(tiles):
        for c in range(2):
            q_send[2 * r + c] = product[
                r * TILE : (r + 1) * TILE, c * LANES : (c + 1) * LANES
            ].astype(BF16)
    q_send[2 * tiles] = stats.astype(BF16)
    copies = exchange("kv", lambda d: q_send, lambda k: q_recv.at[k], q_sems)
    total = total_of(copies, q_send[...].astype(F32), q_recv)
    s = jnp.sum(total[2 * tiles], axis=0, keepdims=True)
    factor = lax.rsqrt(s / (h.shape[1] * n_kv) + EPS)
    factor = jnp.sum(jnp.where(row == lane, factor, 0.0), axis=1, keepdims=True)
    halves = [
        jnp.concatenate([total[2 * r + c] for r in range(tiles)], axis=0) * factor
        for c in range(2)
    ]
    low = lane < HEAD
    first_half = jnp.where(low, halves[0], pltpu.roll(halves[1], HEAD, 1))
    second_half = jnp.where(low, pltpu.roll(halves[0], HEAD, 1), halves[1])
    return first_half.astype(BF16), second_half.astype(BF16)


def spread_queries(q_parts, pairs, qx):
    batch = q_parts[0].shape[0]
    per = qx.shape[1]
    rows = pairs * per
    row = lax.broadcasted_iota(jnp.int32, (rows, batch), 0)
    col = lax.broadcasted_iota(jnp.int32, (rows, batch), 1)
    pick = jnp.where(col == row // per + pairs * lax.rem(row, 2), 1.0, 0.0).astype(BF16)
    wide_row = lax.broadcasted_iota(jnp.int32, (rows, LANES), 0)
    lane = lax.broadcasted_iota(jnp.int32, (rows, LANES), 1)
    which = lax.rem(wide_row // 2, 2)
    y = jnp.where(which == 0, dot(pick, q_parts[0]), dot(pick, q_parts[1]))
    mine = lane // (HEAD // MAPS) == lax.rem(wide_row // 4, 4)
    y = jnp.where(mine, y, 0.0)
    member = lax.rem(wide_row, 2)
    for i in range(2):
        block = jnp.where(member == i, y, 0.0).astype(BF16)
        qx[:, :, i * LANES : (i + 1) * LANES] = block.reshape(pairs, per, LANES)


def attend(scale, qx, k_buf, v_buf, p, o_ref, slot):
    s = lax.dot_general(qx[p], k_buf[p], (((1,), (1,)), ((), ())), preferred_element_type=F32)
    peak = jnp.max(s, axis=1, keepdims=True)
    e = jnp.exp2((s - peak) * scale)
    l = jnp.sum(e, axis=1, keepdims=True)
    o = dot(e.astype(BF16), v_buf[p]) / l
    lse = peak * scale + jnp.log2(l)
    row = lax.broadcasted_iota(jnp.int32, (2 * TILE, LANES), 0)
    lane = lax.broadcasted_iota(jnp.int32, (TILE, LANES), 1)
    o = jnp.where(lax.rem(row, 2) == 0, o[:, :LANES], o[:, LANES:])
    low = lane < HEAD
    o_ref[slot, 0] = jnp.where(low, o[:TILE], o[TILE:])
    o_ref[slot, 1] = jnp.where(low, lse[:TILE], lse[TILE:])


def attention_step(scale, n_kv, qx, k_buf, v_buf, o_send, o_recv, sems):
    order = OFFSETS["kv"]
    copies = []
    for k, offset in enumerate(order):
        dest = shifted("kv", offset)
        attend(scale, qx, k_buf, v_buf, dest, o_send, k)
        copy = pltpu.make_async_remote_copy(
            src_ref=o_send.at[k],
            dst_ref=o_recv.at[k],
            send_sem=sems.at[0, k],
            recv_sem=sems.at[1, k],
            device_id={"kv": dest},
            device_id_type=MESH,
        )
        copy.start()
        copies.append(copy)
    attend(scale, qx, k_buf, v_buf, lax.axis_index("kv"), o_send, len(order))
    return copies


def merge_heads(copies, o_send, o_recv, map_weight, head_gain, group, kv_local):
    for copy in copies:
        copy.wait()
    own = len(copies)
    outs = [o_send[own, 0]] + [o_recv[k, 0] for k in range(own)]
    lses = [o_send[own, 1]] + [o_recv[k, 1] for k in range(own)]
    peak = functools.reduce(jnp.maximum, lses)
    weights = [jnp.exp2(lse - peak) for lse in lses]
    total = functools.reduce(jnp.add, weights)
    merged = functools.reduce(jnp.add, [w * o for w, o in zip(weights, outs)]) / total
    row = lax.broadcasted_iota(jnp.int32, (TILE, LANES), 0)
    lane = lax.broadcasted_iota(jnp.int32, (TILE, LANES), 1)
    weight = jnp.zeros((TILE, LANES), F32)
    for k in range(kv_local):
        for g in range(group):
            here = (lax.rem(row // 2, group) == g) & (lane // HEAD == k)
            at = k * group + g
            weight = jnp.where(here, map_weight[:, at : at + 1], weight)
    diff = merged - weight * pltpu.roll(merged, TILE // 2, 0)
    square = diff * diff
    mean = jnp.zeros((TILE, LANES), F32)
    for k in range(kv_local):
        here = lane // HEAD == k
        mean = jnp.where(here, jnp.sum(jnp.where(here, square, 0.0), axis=1, keepdims=True), mean)
    gain = jnp.concatenate([head_gain[...]] * kv_local, axis=1)
    return diff * lax.rsqrt(mean / HEAD + EPS) * gain * HEAD_SCALE


def start_loads(pairs, sems):
    loads = [pltpu.make_async_copy(a, b, sems.at[i]) for i, (a, b) in enumerate(pairs)]
    for load in loads:
        load.start()
    return loads


def layer_kernel(
    n_kv, n_tp, kv_local, group, scale,
    tokens, first_gain, mix_gain, second_gain, map_weight, head_gain,
    gate1_any, up1_any, down1_any, query_any, key_any, value_any, out_any,
    gate2_any, up2_any, down2_any,
    mixed,
    w_gate1, w_up1, w_down1, w_query, k_buf, v_buf, w_out, w_gate2, w_up2, w_down2,
    tok_all, rs1_send, rs1_recv, act1_own, act1_all, tp1_send, tp1_recv, q_send, q_recv, qx,
    o_send, o_recv, head_own, head_all, tp2_send, tp2_recv,
    rs2_send, rs2_recv, act2_own, act2_all, fin_send, fin_recv,
    load_sems, tok_sems, rs1_sems, ag1_sems, tp1_sems, q_sems, o_sems, head_sems, tp2_sems,
    rs2_sems, ag2_sems, fin_sems,
):
    pairs = k_buf.shape[0]
    chunk = HEAD
    loads = start_loads(
        (
            (gate1_any, w_gate1),
            (up1_any, w_up1),
            (down1_any, w_down1),
            (query_any, w_query),
            (key_any.at[:pairs], k_buf.at[:, :, :LANES]),
            (key_any.at[pairs:], k_buf.at[:, :, LANES:]),
            (value_any.at[:pairs], v_buf.at[:, :, :LANES]),
            (value_any.at[pairs:], v_buf.at[:, :, LANES:]),
            (gate2_any, w_gate2),
            (up2_any, w_up2),
            (down2_any, w_down2),
        )
        + tuple(
            (
                out_any.at[pl.ds((k * group + g) * chunk, chunk)],
                w_out.at[pl.ds((g * kv_local + k) * chunk, chunk)],
            )
            for k in range(kv_local)
            for g in range(group)
        ),
        load_sems,
    )
    greet()
    tp = lax.axis_index("tp")
    me = lax.axis_index("kv")
    tok_all[tp] = tokens[...]
    for copy in exchange("tp", lambda d: tokens, lambda k: tok_all.at[tp], tok_sems):
        copy.wait()
    h = jnp.concatenate([tok_all[j].astype(F32) for j in range(n_tp)], axis=1)
    part = feed_forward(
        n_kv, h, first_gain[...], w_gate1, w_up1, w_down1, loads[:3],
        (rs1_send, rs1_recv, act1_own, act1_all, rs1_sems, ag1_sems),
    )
    h = h + 0.5 * sum_over_tp(part, tp1_send, tp1_recv, tp1_sems)
    loads[3].wait()
    q_parts = query_step(n_kv, h, mix_gain[...], w_query, q_send, q_recv, q_sems)
    spread_queries(q_parts, pairs, qx)
    for load in loads[4:8]:
        load.wait()
    copies = attention_step(scale, n_kv, qx, k_buf, v_buf, o_send, o_recv, o_sems)
    heads = merge_heads(copies, o_send, o_recv, map_weight, head_gain, group, kv_local)
    head_own[...] = heads
    mine = pl.ds(pl.multiple_of(me * TILE, TILE), TILE)
    head_all[mine, :] = heads
    for copy in exchange("kv", lambda d: head_own, lambda k: head_all.at[mine], head_sems):
        copy.wait()
    heads = jnp.concatenate(
        [
            jnp.concatenate(
                [head_all[pl.ds(2 * g + i, pairs, stride=TILE), :] for g in range(group)], axis=1
            )
            for i in range(2)
        ],
        axis=0,
    ).astype(BF16)
    for load in loads[11:]:
        load.wait()
    h = h + sum_over_tp(dot(heads, w_out[...]), tp2_send, tp2_recv, tp2_sems)
    part = feed_forward(
        n_kv, h, second_gain[...], w_gate2, w_up2, w_down2, loads[8:11],
        (rs2_send, rs2_recv, act2_own, act2_all, rs2_sems, ag2_sems),
    )
    batch, width = mixed.shape
    own = jnp.zeros((batch, width), F32)
    for j in range(n_tp):
        columns = slice(j * width, (j + 1) * width)
        fin_send[j] = part[:, columns].astype(BF16)
        own = jnp.where(tp == j, h[:, columns], own)
    copies = exchange("tp", lambda d: fin_send.at[d], lambda k: fin_recv.at[k], fin_sems)
    total = total_of(copies, fin_send[tp].astype(F32), fin_recv)
    mixed[...] = (own + 0.5 * total).astype(BF16)


def dma_sems(n):
    return pltpu.SemaphoreType.DMA((2, n - 1))


def on_device(
    n_kv, n_tp, tokens, first_gain, first_gate, first_up, first_down, mix_gain, w_query,
    key_cache, value_cache, map_weight, head_gain, w_out, second_gain, second_gate, second_up,
    second_down,
):
    batch, own_width = tokens.shape
    depth, hidden = first_gate.shape
    length = key_cache.shape[1]
    columns = w_query.shape[1]
    kv_local = key_cache.shape[2] // HEAD
    group = columns // (kv_local * HEAD)
    pairs = batch // 2
    cw = -(-hidden // (LANES * COL_GROUPS)) * LANES
    vmem = pl.BlockSpec(memory_space=pltpu.VMEM)
    hbm = pl.BlockSpec(memory_space=pl.ANY)
    ffn_buffers = [
        pltpu.VMEM((n_kv, TILE, 2 * cw + LANES), BF16),
        pltpu.VMEM((n_kv - 1, TILE, 2 * cw + LANES), BF16),
        pltpu.VMEM((TILE, cw), BF16),
        pltpu.VMEM((n_kv, TILE, cw), BF16),
    ]
    tp_buffers = [pltpu.VMEM((batch, depth), BF16), pltpu.VMEM((n_tp - 1, batch, depth), BF16)]
    q_tiles = 2 * (batch // TILE) + 1
    return pl.pallas_call(
        functools.partial(
            layer_kernel, n_kv, n_tp, kv_local, group, math.log2(math.e) / math.sqrt(HEAD // MAPS)
        ),
        out_shape=jax.ShapeDtypeStruct((batch, depth // n_tp), BF16),
        in_specs=[vmem] * 6 + [hbm] * 10,
        out_specs=vmem,
        scratch_shapes=[
            pltpu.VMEM(first_gate.shape, BF16),
            pltpu.VMEM(first_up.shape, BF16),
            pltpu.VMEM(first_down.shape, BF16),
            pltpu.VMEM(w_query.shape, BF16),
            pltpu.VMEM((pairs, length, 2 * LANES), BF16),
            pltpu.VMEM((pairs, length, 2 * LANES), BF16),
            pltpu.VMEM(w_out.shape, BF16),
            pltpu.VMEM(second_gate.shape, BF16),
            pltpu.VMEM(second_up.shape, BF16),
            pltpu.VMEM(second_down.shape, BF16),
            pltpu.VMEM((n_tp,) + tokens.shape, BF16),
            *ffn_buffers,
            *tp_buffers,
            pltpu.VMEM((q_tiles, TILE, LANES), BF16),
            pltpu.VMEM((n_kv - 1, q_tiles, TILE, LANES), BF16),
            pltpu.VMEM((pairs, 2 * TILE, 2 * LANES), BF16),
            pltpu.VMEM((n_kv, 2, TILE, LANES), F32),
            pltpu.VMEM((n_kv - 1, 2, TILE, LANES), F32),
            pltpu.VMEM((TILE, LANES), F32),
            pltpu.VMEM((n_kv * TILE, LANES), F32),
            *tp_buffers,
            *ffn_buffers,
            pltpu.VMEM((n_tp, batch, own_width), BF16),
            pltpu.VMEM((n_tp - 1, batch, own_width), BF16),
            pltpu.SemaphoreType.DMA((11 + kv_local * group,)),
            dma_sems(n_tp),
            dma_sems(n_kv),
            dma_sems(n_kv),
            dma_sems(n_tp),
            dma_sems(n_kv),
            dma_sems(n_kv),
            dma_sems(n_kv),
            dma_sems(n_tp),
            dma_sems(n_kv),
            dma_sems(n_kv),
            dma_sems(n_tp),
        ],
        compiler_params=pltpu.CompilerParams(
            collective_id=1, has_side_effects=True, vmem_limit_bytes=VMEM_LIMIT
        ),
    )(
        tokens, first_gain.reshape(1, -1), mix_gain.reshape(1, -1), second_gain.reshape(1, -1),
        map_weight.reshape(1, -1), head_gain.reshape(1, -1),
        first_gate, first_up, first_down, w_query, key_cache, value_cache, w_out,
        second_gate, second_up, second_down,
    )


def solution(mesh):
    placed = (
        P(None, ("kv", "tp")),
        P("kv"),
        P("kv", "tp"),
        P("kv", "tp"),
        P("tp", "kv"),
        P("kv"),
        P("kv", "tp"),
        P(None, "kv", "tp"),
        P(None, "kv", "tp"),
        P("tp"),
        P(),
        P("tp", "kv"),
        P("kv"),
        P("kv", "tp"),
        P("kv", "tp"),
        P("tp", "kv"),
    )
    return jax.shard_map(
        functools.partial(on_device, mesh.shape["kv"], mesh.shape["tp"]),
        mesh=mesh,
        in_specs=placed,
        out_specs=P(None, ("kv", "tp")),
        check_vma=False,
    )
```

time: 101 us -> 74.5 us (0.74)
  Pallas kernels: 94.9 us -> 73 us
  local copies, waits for them, and re-layouts: 4.51 us -> 1.3 us
    pallas_call x3 -> x1, Pallas kernels: 94.9 us -> 73 us  [on_device(): pl.pallas_call(functools.partial(layer_kernel, n_kv, n_tp, kv_local, grou...]
    another operation x4 -> x0, local copies, waits for them, and re-layouts: 1.29 us -> none  [the longest x2 0.68 us: on_device(): weight = jnp.tile(weight, (slab_rows // group, 1))]
where the time goes in v1:
time: 74.5 us; the launch traced here: 74.3 us
  Pallas kernels  73 us (98%)
  local copies, waits for them, and re-layouts  1.3 us (2%)
    pallas_call x1, Pallas kernels, on_device(): pl.pallas_call(functools.partial(layer_kernel, n_kv, n_tp, kv_local, grou...  73 us

profile of v1, /device:TPU:1, one launch (start us, length us, event | category | flops | bytes accessed | tf_op | source)
XLA Modules:
  0.0 74.3 jit_solution(17415712288911553882)
XLA Ops:
  0.0 73.0 %shard_map.154 = bf16[32,32]{1,0:T(8,128)(2,1)} custom-call(bf16[32,32]{1,0:T(8,128)(2,1)} %tokens.1, f32[1,256]{1,0:T(1,128)} %bitcast.5, f32[1,256]{1,0:T(1,128)} %bitcast.6, f32[1,256]{1,0:T(1,128)} %bitcast.7, f32[1,4]{1,0:T(1,128)} %bitcast.8, f32[1,64]{1,0:T(1,128)} %bitcast.9, bf16[256,1408]{1,0:T(8,128)(2,1)} %gate1_any.1, ...), custom_call_target="tpu_custom_call" | custom-call | tf_op jit(solution)/shard_map/pallas_call | solution.py:398
  73.0 1.3 %copy.18 = bf16[32,32]{1,0:T(8,128)(2,1)} copy(bf16[32,32]{1,0:T(8,128)(2,1)} %shard_map.154) | data formatting | bytes 4096

commit v2 on v1

--- a/solution.py
+++ b/solution.py
@@ -17,6 +17,7 @@
 SIDE = 4
 ROW_GROUPS = 4
 COL_GROUPS = 4
+GROUP_ENDS = (5, 10, 14, 16)
 F32 = jnp.float32
 BF16 = jnp.bfloat16
 MESH = pl.DeviceIdType.MESH
@@ -208,51 +209,56 @@
         qx[:, :, i * LANES : (i + 1) * LANES] = block.reshape(pairs, per, LANES)
 
 
-def attend(scale, qx, k_buf, v_buf, p, o_ref, slot):
-    s = lax.dot_general(qx[p], k_buf[p], (((1,), (1,)), ((), ())), preferred_element_type=F32)
-    peak = jnp.max(s, axis=1, keepdims=True)
-    e = jnp.exp2((s - peak) * scale)
-    l = jnp.sum(e, axis=1, keepdims=True)
-    o = dot(e.astype(BF16), v_buf[p]) / l
-    lse = peak * scale + jnp.log2(l)
+def scores(qx, k_buf, p):
+    return lax.dot_general(qx[p], k_buf[p], (((1,), (1,)), ((), ())), preferred_element_type=F32)
+
+
+def attention_step(scale, qx, k_buf, v_buf, o_send, o_recv, st_send, st_recv, o_sems, st_sems):
+    pairs = qx.shape[0]
     row = lax.broadcasted_iota(jnp.int32, (2 * TILE, LANES), 0)
     lane = lax.broadcasted_iota(jnp.int32, (TILE, LANES), 1)
-    o = jnp.where(lax.rem(row, 2) == 0, o[:, :LANES], o[:, LANES:])
+    first_member = lax.rem(row, 2) == 0
     low = lane < HEAD
-    o_ref[slot, 0] = jnp.where(low, o[:TILE], o[TILE:])
-    o_ref[slot, 1] = jnp.where(low, lse[:TILE], lse[TILE:])
-
-
-def attention_step(scale, n_kv, qx, k_buf, v_buf, o_send, o_recv, sems):
-    order = OFFSETS["kv"]
+    stats = jnp.zeros((TILE, LANES), F32)
     copies = []
-    for k, offset in enumerate(order):
-        dest = shifted("kv", offset)
-        attend(scale, qx, k_buf, v_buf, dest, o_send, k)
-        copy = pltpu.make_async_remote_copy(
-            src_ref=o_send.at[k],
-            dst_ref=o_recv.at[k],
-            send_sem=sems.at[0, k],
-            recv_sem=sems.at[1, k],
-            device_id={"kv": dest},
-            device_id_type=MESH,
-        )
-        copy.start()
-        copies.append(copy)
-    attend(scale, qx, k_buf, v_buf, lax.axis_index("kv"), o_send, len(order))
-    return copies
-
-
-def merge_heads(copies, o_send, o_recv, map_weight, head_gain, group, kv_local):
-    for copy in copies:
-        copy.wait()
-    own = len(copies)
-    outs = [o_send[own, 0]] + [o_recv[k, 0] for k in range(own)]
-    lses = [o_send[own, 1]] + [o_recv[k, 1] for k in range(own)]
-    peak = functools.reduce(jnp.maximum, lses)
-    weights = [jnp.exp2(lse - peak) for lse in lses]
-    total = functools.reduce(jnp.add, weights)
-    merged = functools.reduce(jnp.add, [w * o for w, o in zip(weights, outs)]) / total
+    ahead = scores(qx, k_buf, 0)
+    begin = 0
+    for p in range(pairs):
+        s = ahead
+        if p + 1 < pairs:
+            ahead = scores(qx, k_buf, p + 1)
+        peak = jnp.max(s, axis=1, keepdims=True)
+        e = jnp.exp2((s - peak) * scale)
+        l = jnp.sum(e, axis=1, keepdims=True)
+        lse = peak * scale + jnp.log2(l)
+        stats = jnp.where(lane == 2 * p, lse[:TILE], stats)
+        stats = jnp.where(lane == 2 * p + 1, lse[TILE:], stats)
+        o = dot(e.astype(BF16), v_buf[p]) / l
+        o = jnp.where(first_member, o[:, :LANES], o[:, LANES:])
+        o_send[p] = jnp.where(low, o[:TILE], o[TILE:]).astype(BF16)
+        if p + 1 == pairs:
+            st_send[...] = stats
+        if p + 1 in GROUP_ENDS:
+            span = pl.ds(begin, p + 1 - begin)
+            sems = o_sems.at[GROUP_ENDS.index(p + 1)]
+            copies += exchange(
+                "kv", lambda d: o_send.at[span], lambda k: o_recv.at[k, span], sems
+            )
+            begin = p + 1
+    return copies, exchange("kv", lambda d: st_send, lambda k: st_recv.at[k], st_sems)
+
+
+def selector(sel):
+    depth, width = sel.shape
+    for j in range(width // LANES):
+        row = lax.broadcasted_iota(jnp.int32, (depth, LANES), 0)
+        lane = lax.broadcasted_iota(jnp.int32, (depth, LANES), 1)
+        count = width // HEAD
+        here = (lax.rem(row, count) == 2 * j + lane // HEAD) & (row < 2 * count)
+        sel[:, j * LANES : (j + 1) * LANES] = jnp.where(here, 1.0, 0.0).astype(BF16)
+
+
+def head_weights(map_weight, group, kv_local):
     row = lax.broadcasted_iota(jnp.int32, (TILE, LANES), 0)
     lane = lax.broadcasted_iota(jnp.int32, (TILE, LANES), 1)
     weight = jnp.zeros((TILE, LANES), F32)
@@ -261,14 +267,46 @@
             here = (lax.rem(row // 2, group) == g) & (lane // HEAD == k)
             at = k * group + g
             weight = jnp.where(here, map_weight[:, at : at + 1], weight)
-    diff = merged - weight * pltpu.roll(merged, TILE // 2, 0)
-    square = diff * diff
-    mean = jnp.zeros((TILE, LANES), F32)
-    for k in range(kv_local):
-        here = lane // HEAD == k
-        mean = jnp.where(here, jnp.sum(jnp.where(here, square, 0.0), axis=1, keepdims=True), mean)
-    gain = jnp.concatenate([head_gain[...]] * kv_local, axis=1)
-    return diff * lax.rsqrt(mean / HEAD + EPS) * gain * HEAD_SCALE
+    return weight
+
+
+def merge_heads(copies, st_copies, o_send, o_recv, st_send, st_recv, sel, weight, gain, heads):
+    pairs = o_send.shape[0]
+    count = 2 * pairs
+    others = len(st_copies)
+    lane = lax.broadcasted_iota(jnp.int32, (TILE, LANES), 1)
+    for copy in st_copies:
+        copy.wait()
+    lses = [st_send[...]] + [st_recv[k] for k in range(others)]
+    peak = functools.reduce(jnp.maximum, lses)
+    weights = [jnp.exp2(lse - peak) for lse in lses]
+    share = 1.0 / functools.reduce(jnp.add, weights)
+    rows = []
+    for w in weights:
+        w = w * share
+        high = w.astype(BF16).astype(F32)
+        rest = pltpu.roll(w - high, count, 1)
+        rows.append(jnp.where(lane < count, high, jnp.where(lane < 2 * count, rest, 0.0)))
+    spread = jnp.concatenate(rows, axis=0).astype(BF16)
+    for copy in copies:
+        copy.wait()
+    low = lane < HEAD
+    for j in range(pairs // 2):
+        wide = dot(spread, sel[:, 2 * j * LANES : 2 * (j + 1) * LANES])
+        for i in range(2):
+            p = 2 * j + i
+            columns = slice(i * LANES, (i + 1) * LANES)
+            outs = [o_send[p].astype(F32)] + [o_recv[k, p].astype(F32) for k in range(others)]
+            merged = functools.reduce(
+                jnp.add,
+                [wide[d * TILE : (d + 1) * TILE, columns] * o for d, o in enumerate(outs)],
+            )
+            diff = merged - weight * pltpu.roll(merged, TILE // 2, 0)
+            square = diff * diff
+            left = jnp.sum(jnp.where(low, square, 0.0), axis=1, keepdims=True)
+            right = jnp.sum(jnp.where(low, 0.0, square), axis=1, keepdims=True)
+            mean = jnp.where(low, left, right) / HEAD
+            heads[p * TILE : (p + 1) * TILE, :] = diff * lax.rsqrt(mean + EPS) * gain
 
 
 def start_loads(pairs, sems):
@@ -280,19 +318,30 @@
 
 def layer_kernel(
     n_kv, n_tp, kv_local, group, scale,
-    tokens, first_gain, mix_gain, second_gain, map_weight, head_gain,
+    tokens_any, gain1_any, gain_mix_any, gain2_any, weight_any, head_gain_any,
     gate1_any, up1_any, down1_any, query_any, key_any, value_any, out_any,
     gate2_any, up2_any, down2_any,
     mixed,
+    tokens, first_gain, mix_gain, second_gain, map_weight, head_gain,
     w_gate1, w_up1, w_down1, w_query, k_buf, v_buf, w_out, w_gate2, w_up2, w_down2,
     tok_all, rs1_send, rs1_recv, act1_own, act1_all, tp1_send, tp1_recv, q_send, q_recv, qx,
-    o_send, o_recv, head_own, head_all, tp2_send, tp2_recv,
+    o_send, o_recv, st_send, st_recv, sel, head_all, tp2_send, tp2_recv,
     rs2_send, rs2_recv, act2_own, act2_all, fin_send, fin_recv,
-    load_sems, tok_sems, rs1_sems, ag1_sems, tp1_sems, q_sems, o_sems, head_sems, tp2_sems,
-    rs2_sems, ag2_sems, fin_sems,
+    small_sems, load_sems, tok_sems, rs1_sems, ag1_sems, tp1_sems, q_sems, o_sems, st_sems,
+    tp2_sems, rs2_sems, ag2_sems, fin_sems,
 ):
     pairs = k_buf.shape[0]
-    chunk = HEAD
+    small = start_loads(
+        (
+            (tokens_any, tokens),
+            (gain1_any, first_gain),
+            (gain_mix_any, mix_gain),
+            (gain2_any, second_gain),
+            (weight_any, map_weight),
+            (head_gain_any, head_gain),
+        ),
+        small_sems,
+    )
     loads = start_loads(
         (
             (gate1_any, w_gate1),
@@ -309,8 +358,8 @@
         )
         + tuple(
             (
-                out_any.at[pl.ds((k * group + g) * chunk, chunk)],
-                w_out.at[pl.ds((g * kv_local + k) * chunk, chunk)],
+                out_any.at[pl.ds((k * group + g) * HEAD, HEAD)],
+                w_out.at[pl.ds((g * kv_local + k) * HEAD, HEAD)],
             )
             for k in range(kv_local)
             for g in range(group)
@@ -318,10 +367,13 @@
         load_sems,
     )
     greet()
+    for load in small:
+        load.wait()
     tp = lax.axis_index("tp")
-    me = lax.axis_index("kv")
     tok_all[tp] = tokens[...]
-    for copy in exchange("tp", lambda d: tokens, lambda k: tok_all.at[tp], tok_sems):
+    copies = exchange("tp", lambda d: tokens, lambda k: tok_all.at[tp], tok_sems)
+    selector(sel)
+    for copy in copies:
         copy.wait()
     h = jnp.concatenate([tok_all[j].astype(F32) for j in range(n_tp)], axis=1)
     part = feed_forward(
@@ -334,13 +386,14 @@
     spread_queries(q_parts, pairs, qx)
     for load in loads[4:8]:
         load.wait()
-    copies = attention_step(scale, n_kv, qx, k_buf, v_buf, o_send, o_recv, o_sems)
-    heads = merge_heads(copies, o_send, o_recv, map_weight, head_gain, group, kv_local)
-    head_own[...] = heads
-    mine = pl.ds(pl.multiple_of(me * TILE, TILE), TILE)
-    head_all[mine, :] = heads
-    for copy in exchange("kv", lambda d: head_own, lambda k: head_all.at[mine], head_sems):
-        copy.wait()
+    copies, st_copies = attention_step(
+        scale, qx, k_buf, v_buf, o_send, o_recv, st_send, st_recv, o_sems, st_sems
+    )
+    weight = head_weights(map_weight, group, kv_local)
+    gain = jnp.concatenate([head_gain[...] * HEAD_SCALE] * kv_local, axis=1)
+    merge_heads(
+        copies, st_copies, o_send, o_recv, st_send, st_recv, sel, weight, gain, head_all
+    )
     heads = jnp.concatenate(
         [
             jnp.concatenate(
@@ -385,7 +438,6 @@
     group = columns // (kv_local * HEAD)
     pairs = batch // 2
     cw = -(-hidden // (LANES * COL_GROUPS)) * LANES
-    vmem = pl.BlockSpec(memory_space=pltpu.VMEM)
     hbm = pl.BlockSpec(memory_space=pl.ANY)
     ffn_buffers = [
         pltpu.VMEM((n_kv, TILE, 2 * cw + LANES), BF16),
@@ -399,10 +451,16 @@
         functools.partial(
             layer_kernel, n_kv, n_tp, kv_local, group, math.log2(math.e) / math.sqrt(HEAD // MAPS)
         ),
-        out_shape=jax.ShapeDtypeStruct((batch, depth // n_tp), BF16),
-        in_specs=[vmem] * 6 + [hbm] * 10,
-        out_specs=vmem,
+        out_shape=pltpu.VMEM((batch, depth // n_tp), BF16),
+        in_specs=[hbm] * 16,
+        out_specs=pl.BlockSpec(memory_space=pltpu.VMEM),
         scratch_shapes=[
+            pltpu.VMEM(tokens.shape, BF16),
+            pltpu.VMEM((1, depth), F32),
+            pltpu.VMEM((1, depth), F32),
+            pltpu.VMEM((1, depth), F32),
+            pltpu.VMEM((1, kv_local * group), F32),
+            pltpu.VMEM((1, HEAD), F32),
             pltpu.VMEM(first_gate.shape, BF16),
             pltpu.VMEM(first_up.shape, BF16),
             pltpu.VMEM(first_down.shape, BF16),
@@ -419,21 +477,24 @@
             pltpu.VMEM((q_tiles, TILE, LANES), BF16),
             pltpu.VMEM((n_kv - 1, q_tiles, TILE, LANES), BF16),
             pltpu.VMEM((pairs, 2 * TILE, 2 * LANES), BF16),
-            pltpu.VMEM((n_kv, 2, TILE, LANES), F32),
-            pltpu.VMEM((n_kv - 1, 2, TILE, LANES), F32),
+            pltpu.VMEM((pairs, TILE, LANES), BF16),
+            pltpu.VMEM((n_kv - 1, pairs, TILE, LANES), BF16),
             pltpu.VMEM((TILE, LANES), F32),
-            pltpu.VMEM((n_kv * TILE, LANES), F32),
+            pltpu.VMEM((n_kv - 1, TILE, LANES), F32),
+            pltpu.VMEM((LANES, pairs * LANES), BF16),
+            pltpu.VMEM((pairs * TILE, LANES), F32),
             *tp_buffers,
             *ffn_buffers,
             pltpu.VMEM((n_tp, batch, own_width), BF16),
             pltpu.VMEM((n_tp - 1, batch, own_width), BF16),
+            pltpu.SemaphoreType.DMA((6,)),
             pltpu.SemaphoreType.DMA((11 + kv_local * group,)),
             dma_sems(n_tp),
             dma_sems(n_kv),
             dma_sems(n_kv),
             dma_sems(n_tp),
             dma_sems(n_kv),
-            dma_sems(n_kv),
+            pltpu.SemaphoreType.DMA((len(GROUP_ENDS), 2, n_kv - 1)),
             dma_sems(n_kv),
             dma_sems(n_tp),
             dma_sems(n_kv),

time: 74.5 us -> 71 us (0.953)
  Pallas kernels: 73 us -> 70.3 us
    pallas_call x1, Pallas kernels: 73 us -> 70.3 us  [on_device(): pl.pallas_call(functools.partial(layer_kernel, n_kv, n_tp, kv_local, grou...]
where the time goes in v2:
time: 71 us; the launch traced here: 70.9 us
  Pallas kernels  70.3 us (99%)
    pallas_call x1, Pallas kernels, on_device(): pl.pallas_call(functools.partial(layer_kernel, n_kv, n_tp, kv_local, grou...  70.3 us

profile of v2, /device:TPU:1, one launch (start us, length us, event | category | flops | bytes accessed | tf_op | source)
XLA Modules:
  0.0 70.9 jit_solution(4763269100613718635)
XLA Ops:
  0.0 70.3 %shard_map.154 = bf16[32,32]{1,0:T(8,128)(2,1)S(1)} custom-call(bf16[32,32]{1,0:T(8,128)(2,1)} %tokens_any.1, f32[1,256]{1,0:T(1,128)} %bitcast.5, f32[1,256]{1,0:T(1,128)} %bitcast.6, f32[1,256]{1,0:T(1,128)} %bitcast.7, f32[1,4]{1,0:T(1,128)} %bitcast.8, f32[1,64]{1,0:T(1,128)} %bitcast.9, bf16[256,1408]{1,0:T(8,128)(2,1)} %gate1_any.1, ...), custom_call_target="tpu_custom_call" | custom-call | tf_op jit(solution)/shard_map/pallas_call | solution.py:450
  70.3 0.6 copy.18

commit v3 on v2

--- a/solution.py
+++ b/solution.py
@@ -327,7 +327,7 @@
     tok_all, rs1_send, rs1_recv, act1_own, act1_all, tp1_send, tp1_recv, q_send, q_recv, qx,
     o_send, o_recv, st_send, st_recv, sel, head_all, tp2_send, tp2_recv,
     rs2_send, rs2_recv, act2_own, act2_all, fin_send, fin_recv,
-    small_sems, load_sems, tok_sems, rs1_sems, ag1_sems, tp1_sems, q_sems, o_sems, st_sems,
+    small_sems, load_sems, cache_sems, tok_sems, rs1_sems, ag1_sems, tp1_sems, q_sems, o_sems, st_sems,
     tp2_sems, rs2_sems, ag2_sems, fin_sems,
 ):
     pairs = k_buf.shape[0]
@@ -348,10 +348,6 @@
             (up1_any, w_up1),
             (down1_any, w_down1),
             (query_any, w_query),
-            (key_any.at[:pairs], k_buf.at[:, :, :LANES]),
-            (key_any.at[pairs:], k_buf.at[:, :, LANES:]),
-            (value_any.at[:pairs], v_buf.at[:, :, :LANES]),
-            (value_any.at[pairs:], v_buf.at[:, :, LANES:]),
             (gate2_any, w_gate2),
             (up2_any, w_up2),
             (down2_any, w_down2),
@@ -367,6 +363,15 @@
         load_sems,
     )
     greet()
+    cache_loads = start_loads(
+        (
+            (key_any.at[:pairs], k_buf.at[:, :, :LANES]),
+            (key_any.at[pairs:], k_buf.at[:, :, LANES:]),
+            (value_any.at[:pairs], v_buf.at[:, :, :LANES]),
+            (value_any.at[pairs:], v_buf.at[:, :, LANES:]),
+        ),
+        cache_sems,
+    )
     for load in small:
         load.wait()
     tp = lax.axis_index("tp")
@@ -384,7 +389,7 @@
     loads[3].wait()
     q_parts = query_step(n_kv, h, mix_gain[...], w_query, q_send, q_recv, q_sems)
     spread_queries(q_parts, pairs, qx)
-    for load in loads[4:8]:
+    for load in cache_loads:
         load.wait()
     copies, st_copies = attention_step(
         scale, qx, k_buf, v_buf, o_send, o_recv, st_send, st_recv, o_sems, st_sems
@@ -403,11 +408,11 @@
         ],
         axis=0,
     ).astype(BF16)
-    for load in loads[11:]:
+    for load in loads[7:]:
         load.wait()
     h = h + sum_over_tp(dot(heads, w_out[...]), tp2_send, tp2_recv, tp2_sems)
     part = feed_forward(
-        n_kv, h, second_gain[...], w_gate2, w_up2, w_down2, loads[8:11],
+        n_kv, h, second_gain[...], w_gate2, w_up2, w_down2, loads[4:7],
         (rs2_send, rs2_recv, act2_own, act2_all, rs2_sems, ag2_sems),
     )
     batch, width = mixed.shape
@@ -488,7 +493,8 @@
             pltpu.VMEM((n_tp, batch, own_width), BF16),
             pltpu.VMEM((n_tp - 1, batch, own_width), BF16),
             pltpu.SemaphoreType.DMA((6,)),
-            pltpu.SemaphoreType.DMA((11 + kv_local * group,)),
+            pltpu.SemaphoreType.DMA((7 + kv_local * group,)),
+            pltpu.SemaphoreType.DMA((4,)),
             dma_sems(n_tp),
             dma_sems(n_kv),
             dma_sems(n_kv),

time: 71 us -> 67.6 us (0.952)
  Pallas kernels: 70.3 us -> 66.9 us
    pallas_call x1, Pallas kernels: 70.3 us -> 66.9 us  [on_device(): pl.pallas_call(functools.partial(layer_kernel, n_kv, n_tp, kv_local, grou...]
where the time goes in v3:
time: 67.6 us; the launch traced here: 67.5 us
  Pallas kernels  66.9 us (99%)
    pallas_call x1, Pallas kernels, on_device(): pl.pallas_call(functools.partial(layer_kernel, n_kv, n_tp, kv_local, grou...  66.9 us

profile of v3, /device:TPU:1, one launch (start us, length us, event | category | flops | bytes accessed | tf_op | source)
XLA Modules:
  0.0 67.5 jit_solution(1968540401483402050)
XLA Ops:
  0.0 66.9 %shard_map.154 = bf16[32,32]{1,0:T(8,128)(2,1)S(1)} custom-call(bf16[32,32]{1,0:T(8,128)(2,1)} %tokens_any.1, f32[1,256]{1,0:T(1,128)} %bitcast.5, f32[1,256]{1,0:T(1,128)} %bitcast.6, f32[1,256]{1,0:T(1,128)} %bitcast.7, f32[1,4]{1,0:T(1,128)} %bitcast.8, f32[1,64]{1,0:T(1,128)} %bitcast.9, bf16[256,1408]{1,0:T(8,128)(2,1)} %gate1_any.1, ...), custom_call_target="tpu_custom_call" | custom-call | tf_op jit(solution)/shard_map/pallas_call | solution.py:455
  66.9 0.6 copy.18

commit v4 on v3

--- a/solution.py
+++ b/solution.py
@@ -17,7 +17,7 @@
 SIDE = 4
 ROW_GROUPS = 4
 COL_GROUPS = 4
-GROUP_ENDS = (5, 10, 14, 16)
+GROUP_ENDS = (8, 16)
 F32 = jnp.float32
 BF16 = jnp.bfloat16
 MESH = pl.DeviceIdType.MESH
@@ -61,15 +61,15 @@
     pl.semaphore_wait(barrier, total)
 
 
-def exchange(axis, source, target, sems):
+def exchange(axis, source, target, send_sem, recv_sem):
     copies = []
     for k, offset in enumerate(OFFSETS[axis]):
         dest = shifted(axis, offset)
         copy = pltpu.make_async_remote_copy(
             src_ref=source(dest),
             dst_ref=target(k),
-            send_sem=sems.at[0, k],
-            recv_sem=sems.at[1, k],
+            send_sem=send_sem,
+            recv_sem=recv_sem(k),
             device_id={axis: dest},
             device_id_type=MESH,
         )
@@ -78,10 +78,18 @@
     return copies
 
 
+def drain(axis, ref, sem):
+    peer = shifted(axis, OFFSETS[axis][0])
+    pltpu.make_async_remote_copy(
+        src_ref=ref, dst_ref=ref, send_sem=sem, recv_sem=sem,
+        device_id={axis: peer}, device_id_type=MESH,
+    ).wait_recv()
+
+
 def total_of(copies, own, recv):
     total = own
     for k in reversed(range(len(copies))):
-        copies[k].wait()
+        copies[k].wait_recv()
         total = total + recv[k].astype(F32)
     return total
 
@@ -106,8 +114,9 @@
     return lax.rsqrt(s / width + EPS)
 
 
-def feed_forward(n_kv, h, gain, w_gate, w_up, w_down, loads, scratch):
-    send, recv, act_own, act_all, rs_sems, ag_sems = scratch
+def feed_forward(n_kv, h, gain, w_gate, w_up, w_down, loads, scratch, sems, meanwhile):
+    send, recv, act_own, act_all = scratch
+    rs_send, rs_recv, ag_send, ag_recv = sems
     me = lax.axis_index("kv")
     hidden = w_gate.shape[1]
     cw = act_own.shape[1]
@@ -129,7 +138,9 @@
                     )
         for r in range(ROW_GROUPS):
             send[r * COL_GROUPS + c, :, 2 * cw :] = tile[r * TILE : (r + 1) * TILE]
-    copies = exchange("kv", lambda d: send.at[d], lambda k: recv.at[k], rs_sems)
+    copies = exchange(
+        "kv", lambda d: send.at[d], lambda k: recv.at[k], rs_send, lambda k: rs_recv.at[k]
+    )
     total = total_of(copies, send[me].astype(F32), recv)
     factor = row_factor(total[:, 2 * cw :], h.shape[1] * n_kv)
     gate = total[:, :cw] * factor
@@ -137,10 +148,10 @@
     act = (gate / (1.0 + jnp.exp(-gate)) * up).astype(BF16)
     act_own[...] = act
     act_all[me] = act
-    copies = exchange("kv", lambda d: act_own, lambda k: act_all.at[me], ag_sems)
-    for copy in copies:
-        copy.wait()
+    exchange("kv", lambda d: act_own, lambda k: act_all.at[me], ag_send, lambda k: ag_recv)
+    meanwhile()
     loads[2].wait()
+    drain("kv", act_all.at[pl.ds(0, n_kv - 1)], ag_recv)
     out = None
     for c in range(COL_GROUPS):
         low = c * cw
@@ -153,13 +164,17 @@
     return out
 
 
-def sum_over_tp(part, send, recv, sems):
+def sum_over_tp(part, send, recv, send_sem, recv_sems, meanwhile=None):
     send[...] = part.astype(BF16)
-    copies = exchange("tp", lambda d: send, lambda k: recv.at[k], sems)
+    copies = exchange(
+        "tp", lambda d: send, lambda k: recv.at[k], send_sem, lambda k: recv_sems.at[k]
+    )
+    if meanwhile is not None:
+        meanwhile()
     return total_of(copies, send[...].astype(F32), recv)
 
 
-def query_step(n_kv, h, gain, w_query, q_send, q_recv, q_sems):
+def query_step(n_kv, h, gain, w_query, q_send, q_recv, send_sem, recv_sems):
     rows = h.shape[0]
     product = dot((h * gain).astype(BF16), w_query[...])
     row = lax.broadcasted_iota(jnp.int32, (rows, LANES), 0)
@@ -175,7 +190,9 @@
                 r * TILE : (r + 1) * TILE, c * LANES : (c + 1) * LANES
             ].astype(BF16)
     q_send[2 * tiles] = stats.astype(BF16)
-    copies = exchange("kv", lambda d: q_send, lambda k: q_recv.at[k], q_sems)
+    copies = exchange(
+        "kv", lambda d: q_send, lambda k: q_recv.at[k], send_sem, lambda k: recv_sems.at[k]
+    )
     total = total_of(copies, q_send[...].astype(F32), q_recv)
     s = jnp.sum(total[2 * tiles], axis=0, keepdims=True)
     factor = lax.rsqrt(s / (h.shape[1] * n_kv) + EPS)
@@ -209,24 +226,29 @@
         qx[:, :, i * LANES : (i + 1) * LANES] = block.reshape(pairs, per, LANES)
 
 
-def scores(qx, k_buf, p):
-    return lax.dot_general(qx[p], k_buf[p], (((1,), (1,)), ((), ())), preferred_element_type=F32)
-
-
-def attention_step(scale, qx, k_buf, v_buf, o_send, o_recv, st_send, st_recv, o_sems, st_sems):
+def turn_keys(k_buf, k_turned, first, last):
+    def body(p, carry):
+        k_turned[p] = k_buf[p].T
+        return carry
+
+    lax.fori_loop(first, last, body, 0)
+
+
+def attention_step(
+    scale, qx, k_turned, v_buf, o_send, o_recv, st_send, st_recv, send_sems, recv_sems
+):
     pairs = qx.shape[0]
     row = lax.broadcasted_iota(jnp.int32, (2 * TILE, LANES), 0)
     lane = lax.broadcasted_iota(jnp.int32, (TILE, LANES), 1)
     first_member = lax.rem(row, 2) == 0
     low = lane < HEAD
     stats = jnp.zeros((TILE, LANES), F32)
-    copies = []
-    ahead = scores(qx, k_buf, 0)
+    ahead = dot(qx[0], k_turned[0])
     begin = 0
     for p in range(pairs):
         s = ahead
         if p + 1 < pairs:
-            ahead = scores(qx, k_buf, p + 1)
+            ahead = dot(qx[p + 1], k_turned[p + 1])
         peak = jnp.max(s, axis=1, keepdims=True)
         e = jnp.exp2((s - peak) * scale)
         l = jnp.sum(e, axis=1, keepdims=True)
@@ -237,15 +259,26 @@
         o = jnp.where(first_member, o[:, :LANES], o[:, LANES:])
         o_send[p] = jnp.where(low, o[:TILE], o[TILE:]).astype(BF16)
         if p + 1 == pairs:
-            st_send[...] = stats
+            st_send[...] = stats[:, : 2 * pairs]
+            exchange(
+                "kv", lambda d: st_send, lambda k: st_recv.at[k],
+                send_sems.at[0], lambda k: recv_sems.at[0],
+            )
         if p + 1 in GROUP_ENDS:
             span = pl.ds(begin, p + 1 - begin)
-            sems = o_sems.at[GROUP_ENDS.index(p + 1)]
-            copies += exchange(
-                "kv", lambda d: o_send.at[span], lambda k: o_recv.at[k, span], sems
+            at = GROUP_ENDS.index(p + 1) + 1
+            exchange(
+                "kv", lambda d: o_send.at[span], lambda k: o_recv.at[k, span],
+                send_sems.at[at], lambda k: recv_sems.at[at],
             )
             begin = p + 1
-    return copies, exchange("kv", lambda d: st_send, lambda k: st_recv.at[k], st_sems)
+
+
+def drain_groups(o_recv, sems):
+    begin = 0
+    for at, end in enumerate(GROUP_ENDS):
+        drain("kv", o_recv.at[:, pl.ds(begin, end - begin)], sems.at[at + 1])
+        begin = end
 
 
 def selector(sel):
@@ -254,7 +287,7 @@
         row = lax.broadcasted_iota(jnp.int32, (depth, LANES), 0)
         lane = lax.broadcasted_iota(jnp.int32, (depth, LANES), 1)
         count = width // HEAD
-        here = (lax.rem(row, count) == 2 * j + lane // HEAD) & (row < 2 * count)
+        here = lax.rem(row, count) == 2 * j + lane // HEAD
         sel[:, j * LANES : (j + 1) * LANES] = jnp.where(here, 1.0, 0.0).astype(BF16)
 
 
@@ -270,26 +303,21 @@
     return weight
 
 
-def merge_heads(copies, st_copies, o_send, o_recv, st_send, st_recv, sel, weight, gain, heads):
+def merge_heads(o_send, o_recv, st_send, st_recv, recv_sems, sel, weight, gain, heads):
     pairs = o_send.shape[0]
     count = 2 * pairs
-    others = len(st_copies)
+    others = st_recv.shape[0]
     lane = lax.broadcasted_iota(jnp.int32, (TILE, LANES), 1)
-    for copy in st_copies:
-        copy.wait()
+    drain("kv", st_recv, recv_sems.at[0])
     lses = [st_send[...]] + [st_recv[k] for k in range(others)]
     peak = functools.reduce(jnp.maximum, lses)
     weights = [jnp.exp2(lse - peak) for lse in lses]
     share = 1.0 / functools.reduce(jnp.add, weights)
-    rows = []
-    for w in weights:
-        w = w * share
-        high = w.astype(BF16).astype(F32)
-        rest = pltpu.roll(w - high, count, 1)
-        rows.append(jnp.where(lane < count, high, jnp.where(lane < 2 * count, rest, 0.0)))
-    spread = jnp.concatenate(rows, axis=0).astype(BF16)
-    for copy in copies:
-        copy.wait()
+    compact = jnp.concatenate([w * share for w in weights], axis=0)
+    high = compact.astype(BF16)
+    rest = (compact - high.astype(F32)).astype(BF16)
+    spread = jnp.concatenate([high, rest], axis=1)
+    drain_groups(o_recv, recv_sems)
     low = lane < HEAD
     for j in range(pairs // 2):
         wide = dot(spread, sel[:, 2 * j * LANES : 2 * (j + 1) * LANES])
@@ -323,12 +351,12 @@
     gate2_any, up2_any, down2_any,
     mixed,
     tokens, first_gain, mix_gain, second_gain, map_weight, head_gain,
-    w_gate1, w_up1, w_down1, w_query, k_buf, v_buf, w_out, w_gate2, w_up2, w_down2,
+    w_gate1, w_up1, w_down1, w_query, k_buf, k_turned, v_buf, w_out, w_gate2, w_up2, w_down2,
     tok_all, rs1_send, rs1_recv, act1_own, act1_all, tp1_send, tp1_recv, q_send, q_recv, qx,
     o_send, o_recv, st_send, st_recv, sel, head_all, tp2_send, tp2_recv,
     rs2_send, rs2_recv, act2_own, act2_all, fin_send, fin_recv,
-    small_sems, load_sems, cache_sems, tok_sems, rs1_sems, ag1_sems, tp1_sems, q_sems, o_sems, st_sems,
-    tp2_sems, rs2_sems, ag2_sems, fin_sems,
+    small_sems, load_sems, cache_sems, send_sems, once_sems, kv_sems, tp1_sems, tp2_sems,
+    o_send_sems, o_recv_sems,
 ):
     pairs = k_buf.shape[0]
     small = start_loads(
@@ -376,29 +404,41 @@
         load.wait()
     tp = lax.axis_index("tp")
     tok_all[tp] = tokens[...]
-    copies = exchange("tp", lambda d: tokens, lambda k: tok_all.at[tp], tok_sems)
+    exchange(
+        "tp", lambda d: tokens, lambda k: tok_all.at[tp], send_sems.at[0], lambda k: once_sems.at[0]
+    )
     selector(sel)
-    for copy in copies:
-        copy.wait()
+    drain("tp", tok_all.at[pl.ds(0, n_tp - 1)], once_sems.at[0])
     h = jnp.concatenate([tok_all[j].astype(F32) for j in range(n_tp)], axis=1)
+
+    def keys_first():
+        cache_loads[0].wait()
+        cache_loads[1].wait()
+        turn_keys(k_buf, k_turned, 0, pairs // 2)
+
+    def keys_second():
+        turn_keys(k_buf, k_turned, pairs // 2, pairs)
+
     part = feed_forward(
         n_kv, h, first_gain[...], w_gate1, w_up1, w_down1, loads[:3],
-        (rs1_send, rs1_recv, act1_own, act1_all, rs1_sems, ag1_sems),
-    )
-    h = h + 0.5 * sum_over_tp(part, tp1_send, tp1_recv, tp1_sems)
+        (rs1_send, rs1_recv, act1_own, act1_all),
+        (send_sems.at[1], kv_sems, send_sems.at[2], once_sems.at[1]),
+        keys_first,
+    )
+    h = h + 0.5 * sum_over_tp(part, tp1_send, tp1_recv, send_sems.at[3], tp1_sems, keys_second)
     loads[3].wait()
-    q_parts = query_step(n_kv, h, mix_gain[...], w_query, q_send, q_recv, q_sems)
+    q_parts = query_step(
+        n_kv, h, mix_gain[...], w_query, q_send, q_recv, send_sems.at[4], kv_sems
+    )
     spread_queries(q_parts, pairs, qx)
-    for load in cache_loads:
-        load.wait()
-    copies, st_copies = attention_step(
-        scale, qx, k_buf, v_buf, o_send, o_recv, st_send, st_recv, o_sems, st_sems
+    cache_loads[2].wait()
+    cache_loads[3].wait()
+    attention_step(
+        scale, qx, k_turned, v_buf, o_send, o_recv, st_send, st_recv, o_send_sems, o_recv_sems
     )
     weight = head_weights(map_weight, group, kv_local)
     gain = jnp.concatenate([head_gain[...] * HEAD_SCALE] * kv_local, axis=1)
-    merge_heads(
-        copies, st_copies, o_send, o_recv, st_send, st_recv, sel, weight, gain, head_all
-    )
+    merge_heads(o_send, o_recv, st_send, st_recv, o_recv_sems, sel, weight, gain, head_all)
     heads = jnp.concatenate(
         [
             jnp.concatenate(
@@ -410,10 +450,12 @@
     ).astype(BF16)
     for load in loads[7:]:
         load.wait()
-    h = h + sum_over_tp(dot(heads, w_out[...]), tp2_send, tp2_recv, tp2_sems)
+    h = h + sum_over_tp(dot(heads, w_out[...]), tp2_send, tp2_recv, send_sems.at[5], tp2_sems)
     part = feed_forward(
         n_kv, h, second_gain[...], w_gate2, w_up2, w_down2, loads[4:7],
-        (rs2_send, rs2_recv, act2_own, act2_all, rs2_sems, ag2_sems),
+        (rs2_send, rs2_recv, act2_own, act2_all),
+        (send_sems.at[6], kv_sems, send_sems.at[7], once_sems.at[2]),
+        lambda: None,
     )
     batch, width = mixed.shape
     own = jnp.zeros((batch, width), F32)
@@ -421,13 +463,23 @@
         columns = slice(j * width, (j + 1) * width)
         fin_send[j] = part[:, columns].astype(BF16)
         own = jnp.where(tp == j, h[:, columns], own)
-    copies = exchange("tp", lambda d: fin_send.at[d], lambda k: fin_recv.at[k], fin_sems)
+    copies = exchange(
+        "tp", lambda d: fin_send.at[d], lambda k: fin_recv.at[k],
+        send_sems.at[8], lambda k: tp1_sems.at[k],
+    )
+    drain("tp", tok_all.at[pl.ds(0, n_tp - 1)], send_sems.at[0])
+    drain("kv", rs1_recv, send_sems.at[1])
+    drain("kv", act1_all.at[pl.ds(0, n_kv - 1)], send_sems.at[2])
+    drain("tp", tp1_recv, send_sems.at[3])
+    drain("kv", q_recv, send_sems.at[4])
+    drain("kv", st_recv, o_send_sems.at[0])
+    drain_groups(o_recv, o_send_sems)
+    drain("tp", tp2_recv, send_sems.at[5])
+    drain("kv", rs2_recv, send_sems.at[6])
+    drain("kv", act2_all.at[pl.ds(0, n_kv - 1)], send_sems.at[7])
     total = total_of(copies, fin_send[tp].astype(F32), fin_recv)
+    drain("tp", fin_recv, send_sems.at[8])
     mixed[...] = (own + 0.5 * total).astype(BF16)
-
-
-def dma_sems(n):
-    return pltpu.SemaphoreType.DMA((2, n - 1))
 
 
 def on_device(
@@ -471,6 +523,7 @@
             pltpu.VMEM(first_down.shape, BF16),
             pltpu.VMEM(w_query.shape, BF16),
             pltpu.VMEM((pairs, length, 2 * LANES), BF16),
+            pltpu.VMEM((pairs, 2 * LANES, length), BF16),
             pltpu.VMEM((pairs, length, 2 * LANES), BF16),
             pltpu.VMEM(w_out.shape, BF16),
             pltpu.VMEM(second_gate.shape, BF16),
@@ -484,9 +537,9 @@
             pltpu.VMEM((pairs, 2 * TILE, 2 * LANES), BF16),
             pltpu.VMEM((pairs, TILE, LANES), BF16),
             pltpu.VMEM((n_kv - 1, pairs, TILE, LANES), BF16),
-            pltpu.VMEM((TILE, LANES), F32),
-            pltpu.VMEM((n_kv - 1, TILE, LANES), F32),
-            pltpu.VMEM((LANES, pairs * LANES), BF16),
+            pltpu.VMEM((TILE, 2 * pairs), F32),
+            pltpu.VMEM((n_kv - 1, TILE, 2 * pairs), F32),
+            pltpu.VMEM((4 * pairs, pairs * LANES), BF16),
             pltpu.VMEM((pairs * TILE, LANES), F32),
             *tp_buffers,
             *ffn_buffers,
@@ -495,17 +548,13 @@
             pltpu.SemaphoreType.DMA((6,)),
             pltpu.SemaphoreType.DMA((7 + kv_local * group,)),
             pltpu.SemaphoreType.DMA((4,)),
-            dma_sems(n_tp),
-            dma_sems(n_kv),
-            dma_sems(n_kv),
-            dma_sems(n_tp),
-            dma_sems(n_kv),
-            pltpu.SemaphoreType.DMA((len(GROUP_ENDS), 2, n_kv - 1)),
-            dma_sems(n_kv),
-            dma_sems(n_tp),
-            dma_sems(n_kv),
-            dma_sems(n_kv),
-            dma_sems(n_tp),
+            pltpu.SemaphoreType.DMA((9,)),
+            pltpu.SemaphoreType.DMA((3,)),
+            pltpu.SemaphoreType.DMA((n_kv - 1,)),
+            pltpu.SemaphoreType.DMA((n_tp - 1,)),
+            pltpu.SemaphoreType.DMA((n_tp - 1,)),
+            pltpu.SemaphoreType.DMA((len(GROUP_ENDS) + 1,)),
+            pltpu.SemaphoreType.DMA((len(GROUP_ENDS) + 1,)),
         ],
         compiler_params=pltpu.CompilerParams(
             collective_id=1, has_side_effects=True, vmem_limit_bytes=VMEM_LIMIT

time: 67.6 us -> 63.8 us (0.944)
  Pallas kernels: 66.9 us -> 63.1 us
    pallas_call x1, Pallas kernels: 66.9 us -> 63.1 us  [on_device(): pl.pallas_call(functools.partial(layer_kernel, n_kv, n_tp, kv_local, grou...]
where the time goes in v4:
time: 63.8 us; the launch traced here: 63.7 us
  Pallas kernels  63.1 us (99%)
    pallas_call x1, Pallas kernels, on_device(): pl.pallas_call(functools.partial(layer_kernel, n_kv, n_tp, kv_local, grou...  63.1 us

profile of v4, /device:TPU:1, one launch (start us, length us, event | category | flops | bytes accessed | tf_op | source)
XLA Modules:
  0.0 63.7 jit_solution(163077780295361389)
XLA Ops:
  0.0 63.1 %shard_map.154 = bf16[32,32]{1,0:T(8,128)(2,1)S(1)} custom-call(bf16[32,32]{1,0:T(8,128)(2,1)} %tokens_any.1, f32[1,256]{1,0:T(1,128)} %bitcast.5, f32[1,256]{1,0:T(1,128)} %bitcast.6, f32[1,256]{1,0:T(1,128)} %bitcast.7, f32[1,4]{1,0:T(1,128)} %bitcast.8, f32[1,64]{1,0:T(1,128)} %bitcast.9, bf16[256,1408]{1,0:T(8,128)(2,1)} %gate1_any.1, ...), custom_call_target="tpu_custom_call" | custom-call | tf_op jit(solution)/shard_map/pallas_call | solution.py:507
  63.1 0.6 copy.18

commit v5 on v4

--- a/solution.py
+++ b/solution.py
@@ -15,9 +15,9 @@
 EPS = 1e-06
 HEAD_SCALE = 0.8
 SIDE = 4
+STEPS = (2, 1, 3, 0)
 ROW_GROUPS = 4
 COL_GROUPS = 4
-GROUP_ENDS = (8, 16)
 F32 = jnp.float32
 BF16 = jnp.bfloat16
 MESH = pl.DeviceIdType.MESH
@@ -118,29 +118,40 @@
     send, recv, act_own, act_all = scratch
     rs_send, rs_recv, ag_send, ag_recv = sems
     me = lax.axis_index("kv")
-    hidden = w_gate.shape[1]
+    hidden = w_down.shape[0]
     cw = act_own.shape[1]
     tile = squares_tile(h)
     scaled = (h * gain).astype(BF16)
     loads[0].wait()
     loads[1].wait()
-    for c in range(COL_GROUPS):
-        low = c * cw
-        w = min(cw, hidden - low)
-        for base, weight in ((0, w_gate), (cw, w_up)):
-            part = dot(scaled, weight[:, low : low + w])
-            for r in range(ROW_GROUPS):
-                rows = slice(r * TILE, (r + 1) * TILE)
-                send[r * COL_GROUPS + c, :, base : base + w] = part[rows].astype(BF16)
-                if w < cw:
-                    send[r * COL_GROUPS + c, :, base + w : base + cw] = jnp.zeros(
-                        (TILE, cw - w), BF16
-                    )
+
+    def product(c):
+        columns = pl.ds(pl.multiple_of(c * cw, LANES), cw)
+        return dot(scaled, jnp.concatenate([w_gate[:, columns], w_up[:, columns]], axis=1))
+
+    z, y = me // SIDE, lax.rem(me, SIDE)
+    groups = [lax.rem(y + step, SIDE) for step in STEPS]
+    copies = [None] * len(OFFSETS["kv"])
+    ahead = product(groups[0])
+    for at, step in enumerate(STEPS):
+        c, part = groups[at], ahead
+        if at + 1 < len(STEPS):
+            ahead = product(groups[at + 1])
         for r in range(ROW_GROUPS):
-            send[r * COL_GROUPS + c, :, 2 * cw :] = tile[r * TILE : (r + 1) * TILE]
-    copies = exchange(
-        "kv", lambda d: send.at[d], lambda k: recv.at[k], rs_send, lambda k: rs_recv.at[k]
-    )
+            rows = slice(r * TILE, (r + 1) * TILE)
+            send[r * COL_GROUPS + c, :, : 2 * cw] = part[rows].astype(BF16)
+            send[r * COL_GROUPS + c, :, 2 * cw :] = tile[rows]
+        for up in STEPS:
+            if (up, step) == (0, 0):
+                continue
+            k = OFFSETS["kv"].index((up, step))
+            dest = lax.rem(z + up, SIDE) * SIDE + c
+            copies[k] = pltpu.make_async_remote_copy(
+                src_ref=send.at[dest], dst_ref=recv.at[k],
+                send_sem=rs_send, recv_sem=rs_recv.at[k],
+                device_id={"kv": dest}, device_id_type=MESH,
+            )
+            copies[k].start()
     total = total_of(copies, send[me].astype(F32), recv)
     factor = row_factor(total[:, 2 * cw :], h.shape[1] * n_kv)
     gate = total[:, :cw] * factor
@@ -174,7 +185,7 @@
     return total_of(copies, send[...].astype(F32), recv)
 
 
-def query_step(n_kv, h, gain, w_query, q_send, q_recv, send_sem, recv_sems):
+def query_step(n_kv, h, gain, w_query, q_send, q_recv, send_sems, recv_sems):
     rows = h.shape[0]
     product = dot((h * gain).astype(BF16), w_query[...])
     row = lax.broadcasted_iota(jnp.int32, (rows, LANES), 0)
@@ -183,37 +194,54 @@
     high = s.astype(BF16).astype(F32)
     first = lax.broadcasted_iota(jnp.int32, (TILE, LANES), 0)
     stats = jnp.where(first == 0, high, jnp.where(first == 1, s - high, 0.0))
-    tiles = rows // TILE
-    for r in range(tiles):
-        for c in range(2):
-            q_send[2 * r + c] = product[
-                r * TILE : (r + 1) * TILE, c * LANES : (c + 1) * LANES
-            ].astype(BF16)
-    q_send[2 * tiles] = stats.astype(BF16)
-    copies = exchange(
-        "kv", lambda d: q_send, lambda k: q_recv.at[k], send_sem, lambda k: recv_sems.at[k]
-    )
-    total = total_of(copies, q_send[...].astype(F32), q_recv)
-    s = jnp.sum(total[2 * tiles], axis=0, keepdims=True)
-    factor = lax.rsqrt(s / (h.shape[1] * n_kv) + EPS)
-    factor = jnp.sum(jnp.where(row == lane, factor, 0.0), axis=1, keepdims=True)
-    halves = [
-        jnp.concatenate([total[2 * r + c] for r in range(tiles)], axis=0) * factor
-        for c in range(2)
+    per = rows // TILE // 2
+    count = 2 * per
+    starts = (0, count + 1)
+    spans = (pl.ds(0, count + 1), pl.ds(count + 1, count))
+    for half in range(2):
+        for r in range(per):
+            for c in range(2):
+                at = (half * per + r) * TILE
+                q_send[starts[half] + 2 * r + c] = product[
+                    at : at + TILE, c * LANES : (c + 1) * LANES
+                ].astype(BF16)
+    q_send[count] = stats.astype(BF16)
+    rounds = [
+        exchange(
+            "kv", lambda d: q_send.at[spans[half]], lambda k: q_recv.at[k, spans[half]],
+            send_sems[half], lambda k: recv_sems[half].at[k],
+        )
+        for half in range(2)
     ]
-    low = lane < HEAD
-    first_half = jnp.where(low, halves[0], pltpu.roll(halves[1], HEAD, 1))
-    second_half = jnp.where(low, pltpu.roll(halves[0], HEAD, 1), halves[1])
-    return first_half.astype(BF16), second_half.astype(BF16)
-
-
-def spread_queries(q_parts, pairs, qx):
+
+    def finish(half, factor):
+        total = total_of(
+            rounds[half], q_send[spans[half]].astype(F32), q_recv.at[:, spans[half]]
+        )
+        if half == 0:
+            s = jnp.sum(total[count], axis=0, keepdims=True)
+            factor = lax.rsqrt(s / (h.shape[1] * n_kv) + EPS)
+            factor = jnp.sum(jnp.where(row == lane, factor, 0.0), axis=1, keepdims=True)
+        mine = factor[half * per * TILE : (half + 1) * per * TILE]
+        parts = [
+            jnp.concatenate([total[2 * r + c] for r in range(per)], axis=0) * mine
+            for c in range(2)
+        ]
+        low = lane[: per * TILE] < HEAD
+        first_half = jnp.where(low, parts[0], pltpu.roll(parts[1], HEAD, 1))
+        second_half = jnp.where(low, pltpu.roll(parts[0], HEAD, 1), parts[1])
+        return (first_half.astype(BF16), second_half.astype(BF16)), factor
+
+    return finish
+
+
+def spread_queries(q_parts, qx, begin, count):
     batch = q_parts[0].shape[0]
     per = qx.shape[1]
-    rows = pairs * per
+    rows = count * per
     row = lax.broadcasted_iota(jnp.int32, (rows, batch), 0)
     col = lax.broadcasted_iota(jnp.int32, (rows, batch), 1)
-    pick = jnp.where(col == row // per + pairs * lax.rem(row, 2), 1.0, 0.0).astype(BF16)
+    pick = jnp.where(col == row // per + count * lax.rem(row, 2), 1.0, 0.0).astype(BF16)
     wide_row = lax.broadcasted_iota(jnp.int32, (rows, LANES), 0)
     lane = lax.broadcasted_iota(jnp.int32, (rows, LANES), 1)
     which = lax.rem(wide_row // 2, 2)
@@ -223,7 +251,9 @@
     member = lax.rem(wide_row, 2)
     for i in range(2):
         block = jnp.where(member == i, y, 0.0).astype(BF16)
-        qx[:, :, i * LANES : (i + 1) * LANES] = block.reshape(pairs, per, LANES)
+        qx[begin : begin + count, :, i * LANES : (i + 1) * LANES] = block.reshape(
+            count, per, LANES
+        )
 
 
 def turn_keys(k_buf, k_turned, first, last):
@@ -234,20 +264,15 @@
     lax.fori_loop(first, last, body, 0)
 
 
-def attention_step(
-    scale, qx, k_turned, v_buf, o_send, o_recv, st_send, st_recv, send_sems, recv_sems
-):
-    pairs = qx.shape[0]
+def attention_step(scale, qx, k_turned, v_buf, begin, end, stats, o_send):
     row = lax.broadcasted_iota(jnp.int32, (2 * TILE, LANES), 0)
     lane = lax.broadcasted_iota(jnp.int32, (TILE, LANES), 1)
     first_member = lax.rem(row, 2) == 0
     low = lane < HEAD
-    stats = jnp.zeros((TILE, LANES), F32)
-    ahead = dot(qx[0], k_turned[0])
-    begin = 0
-    for p in range(pairs):
+    ahead = dot(qx[begin], k_turned[begin])
+    for p in range(begin, end):
         s = ahead
-        if p + 1 < pairs:
+        if p + 1 < end:
             ahead = dot(qx[p + 1], k_turned[p + 1])
         peak = jnp.max(s, axis=1, keepdims=True)
         e = jnp.exp2((s - peak) * scale)
@@ -258,27 +283,13 @@
         o = dot(e.astype(BF16), v_buf[p]) / l
         o = jnp.where(first_member, o[:, :LANES], o[:, LANES:])
         o_send[p] = jnp.where(low, o[:TILE], o[TILE:]).astype(BF16)
-        if p + 1 == pairs:
-            st_send[...] = stats[:, : 2 * pairs]
-            exchange(
-                "kv", lambda d: st_send, lambda k: st_recv.at[k],
-                send_sems.at[0], lambda k: recv_sems.at[0],
-            )
-        if p + 1 in GROUP_ENDS:
-            span = pl.ds(begin, p + 1 - begin)
-            at = GROUP_ENDS.index(p + 1) + 1
-            exchange(
-                "kv", lambda d: o_send.at[span], lambda k: o_recv.at[k, span],
-                send_sems.at[at], lambda k: recv_sems.at[at],
-            )
-            begin = p + 1
+    return stats
 
 
 def drain_groups(o_recv, sems):
-    begin = 0
-    for at, end in enumerate(GROUP_ENDS):
-        drain("kv", o_recv.at[:, pl.ds(begin, end - begin)], sems.at[at + 1])
-        begin = end
+    half = o_recv.shape[1] // 2
+    for i in range(2):
+        drain("kv", o_recv.at[:, pl.ds(i * half, half)], sems.at[i + 1])
 
 
 def selector(sel):
@@ -355,10 +366,12 @@
     tok_all, rs1_send, rs1_recv, act1_own, act1_all, tp1_send, tp1_recv, q_send, q_recv, qx,
     o_send, o_recv, st_send, st_recv, sel, head_all, tp2_send, tp2_recv,
     rs2_send, rs2_recv, act2_own, act2_all, fin_send, fin_recv,
-    small_sems, load_sems, cache_sems, send_sems, once_sems, kv_sems, tp1_sems, tp2_sems,
+    small_sems, load_sems, cache_sems, send_sems, once_sems, kv_sems, second_sems, tp1_sems, tp2_sems,
     o_send_sems, o_recv_sems,
 ):
     pairs = k_buf.shape[0]
+    half = pairs // 2
+    hidden = w_down1.shape[0]
     small = start_loads(
         (
             (tokens_any, tokens),
@@ -372,12 +385,12 @@
     )
     loads = start_loads(
         (
-            (gate1_any, w_gate1),
-            (up1_any, w_up1),
+            (gate1_any, w_gate1.at[:, pl.ds(0, hidden)]),
+            (up1_any, w_up1.at[:, pl.ds(0, hidden)]),
             (down1_any, w_down1),
             (query_any, w_query),
-            (gate2_any, w_gate2),
-            (up2_any, w_up2),
+            (gate2_any, w_gate2.at[:, pl.ds(0, hidden)]),
+            (up2_any, w_up2.at[:, pl.ds(0, hidden)]),
             (down2_any, w_down2),
         )
         + tuple(
@@ -390,13 +403,16 @@
         ),
         load_sems,
     )
+    if hidden < w_gate1.shape[1]:
+        for weight in (w_gate1, w_up1, w_gate2, w_up2):
+            weight[:, hidden:] = jnp.zeros((weight.shape[0], weight.shape[1] - hidden), BF16)
     greet()
     cache_loads = start_loads(
-        (
-            (key_any.at[:pairs], k_buf.at[:, :, :LANES]),
-            (key_any.at[pairs:], k_buf.at[:, :, LANES:]),
-            (value_any.at[:pairs], v_buf.at[:, :, :LANES]),
-            (value_any.at[pairs:], v_buf.at[:, :, LANES:]),
+        tuple(
+            (cache.at[pl.ds((2 * a + i) * half, half)], buf.at[pl.ds(a * half, half), :, lanes])
+            for cache, buf in ((key_any, k_buf), (value_any, v_buf))
+            for a in range(2)
+            for i, lanes in enumerate((pl.ds(0, LANES), pl.ds(LANES, LANES)))
         ),
         cache_sems,
     )
@@ -414,10 +430,12 @@
     def keys_first():
         cache_loads[0].wait()
         cache_loads[1].wait()
-        turn_keys(k_buf, k_turned, 0, pairs // 2)
+        turn_keys(k_buf, k_turned, 0, half)
 
     def keys_second():
-        turn_keys(k_buf, k_turned, pairs // 2, pairs)
+        cache_loads[2].wait()
+        cache_loads[3].wait()
+        turn_keys(k_buf, k_turned, half, pairs)
 
     part = feed_forward(
         n_kv, h, first_gain[...], w_gate1, w_up1, w_down1, loads[:3],
@@ -427,23 +445,43 @@
     )
     h = h + 0.5 * sum_over_tp(part, tp1_send, tp1_recv, send_sems.at[3], tp1_sems, keys_second)
     loads[3].wait()
-    q_parts = query_step(
-        n_kv, h, mix_gain[...], w_query, q_send, q_recv, send_sems.at[4], kv_sems
-    )
-    spread_queries(q_parts, pairs, qx)
-    cache_loads[2].wait()
-    cache_loads[3].wait()
-    attention_step(
-        scale, qx, k_turned, v_buf, o_send, o_recv, st_send, st_recv, o_send_sems, o_recv_sems
-    )
+    finish = query_step(
+        n_kv, h, mix_gain[...], w_query, q_send, q_recv,
+        (send_sems.at[4], send_sems.at[9]), (kv_sems, second_sems),
+    )
+    stats = jnp.zeros((TILE, LANES), F32)
+    factor = None
+    for a in range(2):
+        q_parts, factor = finish(a, factor)
+        begin, end = a * half, (a + 1) * half
+        spread_queries(q_parts, qx, begin, half)
+        cache_loads[4 + 2 * a].wait()
+        cache_loads[5 + 2 * a].wait()
+        stats = attention_step(scale, qx, k_turned, v_buf, begin, end, stats, o_send)
+        if a == 1:
+            st_send[...] = stats[:, : 2 * pairs]
+            exchange(
+                "kv", lambda d: st_send, lambda k: st_recv.at[k],
+                o_send_sems.at[0], lambda k: o_recv_sems.at[0],
+            )
+        span = pl.ds(begin, half)
+        exchange(
+            "kv", lambda d: o_send.at[span], lambda k: o_recv.at[k, span],
+            o_send_sems.at[a + 1], lambda k: o_recv_sems.at[a + 1],
+        )
     weight = head_weights(map_weight, group, kv_local)
     gain = jnp.concatenate([head_gain[...] * HEAD_SCALE] * kv_local, axis=1)
     merge_heads(o_send, o_recv, st_send, st_recv, o_recv_sems, sel, weight, gain, head_all)
     heads = jnp.concatenate(
         [
             jnp.concatenate(
-                [head_all[pl.ds(2 * g + i, pairs, stride=TILE), :] for g in range(group)], axis=1
+                [
+                    head_all[pl.ds(a * half * TILE + 2 * g + i, half, stride=TILE), :]
+                    for g in range(group)
+                ],
+                axis=1,
             )
+            for a in range(2)
             for i in range(2)
         ],
         axis=0,
@@ -471,7 +509,9 @@
     drain("kv", rs1_recv, send_sems.at[1])
     drain("kv", act1_all.at[pl.ds(0, n_kv - 1)], send_sems.at[2])
     drain("tp", tp1_recv, send_sems.at[3])
-    drain("kv", q_recv, send_sems.at[4])
+    split = q_recv.shape[1] // 2 + 1
+    drain("kv", q_recv.at[:, pl.ds(0, split)], send_sems.at[4])
+    drain("kv", q_recv.at[:, pl.ds(split, split - 1)], send_sems.at[9])
     drain("kv", st_recv, o_send_sems.at[0])
     drain_groups(o_recv, o_send_sems)
     drain("tp", tp2_recv, send_sems.at[5])
@@ -518,16 +558,16 @@
             pltpu.VMEM((1, depth), F32),
             pltpu.VMEM((1, kv_local * group), F32),
             pltpu.VMEM((1, HEAD), F32),
-            pltpu.VMEM(first_gate.shape, BF16),
-            pltpu.VMEM(first_up.shape, BF16),
+            pltpu.VMEM((depth, COL_GROUPS * cw), BF16),
+            pltpu.VMEM((depth, COL_GROUPS * cw), BF16),
             pltpu.VMEM(first_down.shape, BF16),
             pltpu.VMEM(w_query.shape, BF16),
             pltpu.VMEM((pairs, length, 2 * LANES), BF16),
             pltpu.VMEM((pairs, 2 * LANES, length), BF16),
             pltpu.VMEM((pairs, length, 2 * LANES), BF16),
             pltpu.VMEM(w_out.shape, BF16),
-            pltpu.VMEM(second_gate.shape, BF16),
-            pltpu.VMEM(second_up.shape, BF16),
+            pltpu.VMEM((depth, COL_GROUPS * cw), BF16),
+            pltpu.VMEM((depth, COL_GROUPS * cw), BF16),
             pltpu.VMEM(second_down.shape, BF16),
             pltpu.VMEM((n_tp,) + tokens.shape, BF16),
             *ffn_buffers,
@@ -547,14 +587,15 @@
             pltpu.VMEM((n_tp - 1, batch, own_width), BF16),
             pltpu.SemaphoreType.DMA((6,)),
             pltpu.SemaphoreType.DMA((7 + kv_local * group,)),
-            pltpu.SemaphoreType.DMA((4,)),
-            pltpu.SemaphoreType.DMA((9,)),
+            pltpu.SemaphoreType.DMA((8,)),
+            pltpu.SemaphoreType.DMA((10,)),
             pltpu.SemaphoreType.DMA((3,)),
+            pltpu.SemaphoreType.DMA((n_kv - 1,)),
             pltpu.SemaphoreType.DMA((n_kv - 1,)),
             pltpu.SemaphoreType.DMA((n_tp - 1,)),
             pltpu.SemaphoreType.DMA((n_tp - 1,)),
-            pltpu.SemaphoreType.DMA((len(GROUP_ENDS) + 1,)),
-            pltpu.SemaphoreType.DMA((len(GROUP_ENDS) + 1,)),
+            pltpu.SemaphoreType.DMA((3,)),
+            pltpu.SemaphoreType.DMA((3,)),
         ],
         compiler_params=pltpu.CompilerParams(
             collective_id=1, has_side_effects=True, vmem_limit_bytes=VMEM_LIMIT

time: 63.8 us -> 62.7 us (0.983)
  Pallas kernels: 63.1 us -> 62 us
    pallas_call x1, Pallas kernels: 63.1 us -> 62 us  [on_device(): pl.pallas_call(functools.partial(layer_kernel, n_kv, n_tp, kv_local, grou...]
where the time goes in v5:
time: 62.7 us; the launch traced here: 62.6 us
  Pallas kernels  62 us (99%)
    pallas_call x1, Pallas kernels, on_device(): pl.pallas_call(functools.partial(layer_kernel, n_kv, n_tp, kv_local, grou...  62 us

profile of v5, /device:TPU:1, one launch (start us, length us, event | category | flops | bytes accessed | tf_op | source)
XLA Modules:
  0.0 62.6 jit_solution(18233897830684201608)
XLA Ops:
  0.0 62.0 %shard_map.154 = bf16[32,32]{1,0:T(8,128)(2,1)S(1)} custom-call(bf16[32,32]{1,0:T(8,128)(2,1)} %tokens_any.1, f32[1,256]{1,0:T(1,128)} %bitcast.5, f32[1,256]{1,0:T(1,128)} %bitcast.6, f32[1,256]{1,0:T(1,128)} %bitcast.7, f32[1,4]{1,0:T(1,128)} %bitcast.8, f32[1,64]{1,0:T(1,128)} %bitcast.9, bf16[256,1408]{1,0:T(8,128)(2,1)} %gate1_any.1, ...), custom_call_target="tpu_custom_call" | custom-call | tf_op jit(solution)/shard_map/pallas_call | solution.py:547
  62.0 0.6 copy.18

commit v6 on v5

--- a/solution.py
+++ b/solution.py
@@ -264,11 +264,12 @@
     lax.fori_loop(first, last, body, 0)
 
 
-def attention_step(scale, qx, k_turned, v_buf, begin, end, stats, o_send):
+def attention_step(scale, qx, k_turned, v_buf, begin, end, o_send):
     row = lax.broadcasted_iota(jnp.int32, (2 * TILE, LANES), 0)
     lane = lax.broadcasted_iota(jnp.int32, (TILE, LANES), 1)
     first_member = lax.rem(row, 2) == 0
     low = lane < HEAD
+    stats = jnp.zeros((TILE, LANES), F32)
     ahead = dot(qx[begin], k_turned[begin])
     for p in range(begin, end):
         s = ahead
@@ -278,18 +279,25 @@
         e = jnp.exp2((s - peak) * scale)
         l = jnp.sum(e, axis=1, keepdims=True)
         lse = peak * scale + jnp.log2(l)
-        stats = jnp.where(lane == 2 * p, lse[:TILE], stats)
-        stats = jnp.where(lane == 2 * p + 1, lse[TILE:], stats)
+        stats = jnp.where(lane == 2 * (p - begin), lse[:TILE], stats)
+        stats = jnp.where(lane == 2 * (p - begin) + 1, lse[TILE:], stats)
         o = dot(e.astype(BF16), v_buf[p]) / l
         o = jnp.where(first_member, o[:, :LANES], o[:, LANES:])
         o_send[p] = jnp.where(low, o[:TILE], o[TILE:]).astype(BF16)
     return stats
 
 
-def drain_groups(o_recv, sems):
-    half = o_recv.shape[1] // 2
-    for i in range(2):
-        drain("kv", o_recv.at[:, pl.ds(i * half, half)], sems.at[i + 1])
+def split_three(x, width):
+    high = x.astype(BF16).astype(F32)
+    rest = x - high
+    middle = rest.astype(BF16).astype(F32)
+    low = rest - middle
+    return (high + pltpu.roll(middle, width, 1) + pltpu.roll(low, 2 * width, 1)).astype(BF16)
+
+
+def join_three(tile, width):
+    x = tile.astype(F32)
+    return x + pltpu.roll(x, LANES - width, 1) + pltpu.roll(x, LANES - 2 * width, 1)
 
 
 def selector(sel):
@@ -314,26 +322,27 @@
     return weight
 
 
-def merge_heads(o_send, o_recv, st_send, st_recv, recv_sems, sel, weight, gain, heads):
-    pairs = o_send.shape[0]
-    count = 2 * pairs
+def merge_heads(a, o_send, o_recv, st_send, st_recv, recv_sems, sel, weight, gain, heads):
+    half = o_send.shape[0] // 2
+    count = 2 * half
     others = st_recv.shape[0]
     lane = lax.broadcasted_iota(jnp.int32, (TILE, LANES), 1)
-    drain("kv", st_recv, recv_sems.at[0])
-    lses = [st_send[...]] + [st_recv[k] for k in range(others)]
+    drain("kv", st_recv.at[:, a], recv_sems.at[a])
+    lses = [join_three(st_send[a], count)]
+    lses += [join_three(st_recv[k, a], count) for k in range(others)]
     peak = functools.reduce(jnp.maximum, lses)
     weights = [jnp.exp2(lse - peak) for lse in lses]
     share = 1.0 / functools.reduce(jnp.add, weights)
-    compact = jnp.concatenate([w * share for w in weights], axis=0)
+    compact = jnp.concatenate([w * share for w in weights], axis=0)[:, :count]
     high = compact.astype(BF16)
     rest = (compact - high.astype(F32)).astype(BF16)
     spread = jnp.concatenate([high, rest], axis=1)
-    drain_groups(o_recv, recv_sems)
+    drain("kv", o_recv.at[:, pl.ds(a * half, half)], recv_sems.at[2 + a])
     low = lane < HEAD
-    for j in range(pairs // 2):
+    for j in range(half // 2):
         wide = dot(spread, sel[:, 2 * j * LANES : 2 * (j + 1) * LANES])
         for i in range(2):
-            p = 2 * j + i
+            p = a * half + 2 * j + i
             columns = slice(i * LANES, (i + 1) * LANES)
             outs = [o_send[p].astype(F32)] + [o_recv[k, p].astype(F32) for k in range(others)]
             merged = functools.reduce(
@@ -366,7 +375,7 @@
     tok_all, rs1_send, rs1_recv, act1_own, act1_all, tp1_send, tp1_recv, q_send, q_recv, qx,
     o_send, o_recv, st_send, st_recv, sel, head_all, tp2_send, tp2_recv,
     rs2_send, rs2_recv, act2_own, act2_all, fin_send, fin_recv,
-    small_sems, load_sems, cache_sems, send_sems, once_sems, kv_sems, second_sems, tp1_sems, tp2_sems,
+    small_sems, load_sems, cache_sems, send_sems, once_sems, kv_sems, second_sems, tp1_sems, tp2_sems, tp2_more_sems,
     o_send_sems, o_recv_sems,
 ):
     pairs = k_buf.shape[0]
@@ -449,7 +458,6 @@
         n_kv, h, mix_gain[...], w_query, q_send, q_recv,
         (send_sems.at[4], send_sems.at[9]), (kv_sems, second_sems),
     )
-    stats = jnp.zeros((TILE, LANES), F32)
     factor = None
     for a in range(2):
         q_parts, factor = finish(a, factor)
@@ -457,38 +465,51 @@
         spread_queries(q_parts, qx, begin, half)
         cache_loads[4 + 2 * a].wait()
         cache_loads[5 + 2 * a].wait()
-        stats = attention_step(scale, qx, k_turned, v_buf, begin, end, stats, o_send)
-        if a == 1:
-            st_send[...] = stats[:, : 2 * pairs]
-            exchange(
-                "kv", lambda d: st_send, lambda k: st_recv.at[k],
-                o_send_sems.at[0], lambda k: o_recv_sems.at[0],
-            )
+        stats = attention_step(scale, qx, k_turned, v_buf, begin, end, o_send)
+        st_send[a] = split_three(stats, 2 * half)
+        exchange(
+            "kv", lambda d: st_send.at[a], lambda k: st_recv.at[k, a],
+            o_send_sems.at[a], lambda k: o_recv_sems.at[a],
+        )
         span = pl.ds(begin, half)
         exchange(
             "kv", lambda d: o_send.at[span], lambda k: o_recv.at[k, span],
-            o_send_sems.at[a + 1], lambda k: o_recv_sems.at[a + 1],
+            o_send_sems.at[2 + a], lambda k: o_recv_sems.at[2 + a],
         )
     weight = head_weights(map_weight, group, kv_local)
     gain = jnp.concatenate([head_gain[...] * HEAD_SCALE] * kv_local, axis=1)
-    merge_heads(o_send, o_recv, st_send, st_recv, o_recv_sems, sel, weight, gain, head_all)
-    heads = jnp.concatenate(
-        [
-            jnp.concatenate(
-                [
-                    head_all[pl.ds(a * half * TILE + 2 * g + i, half, stride=TILE), :]
-                    for g in range(group)
-                ],
-                axis=1,
-            )
-            for a in range(2)
-            for i in range(2)
-        ],
-        axis=0,
-    ).astype(BF16)
     for load in loads[7:]:
         load.wait()
-    h = h + sum_over_tp(dot(heads, w_out[...]), tp2_send, tp2_recv, send_sems.at[5], tp2_sems)
+    rounds = []
+    for a in range(2):
+        merge_heads(a, o_send, o_recv, st_send, st_recv, o_recv_sems, sel, weight, gain, head_all)
+        heads = jnp.concatenate(
+            [
+                jnp.concatenate(
+                    [
+                        head_all[pl.ds(a * half * TILE + 2 * g + i, half, stride=TILE), :]
+                        for g in range(group)
+                    ],
+                    axis=1,
+                )
+                for i in range(2)
+            ],
+            axis=0,
+        ).astype(BF16)
+        span = pl.ds(2 * a * half, 2 * half)
+        tp2_send[span, :] = dot(heads, w_out[...]).astype(BF16)
+        sems = (tp2_sems, tp2_more_sems)[a]
+        rounds.append(
+            exchange(
+                "tp", lambda d: tp2_send.at[span], lambda k: tp2_recv.at[k, span],
+                send_sems.at[5 * (a + 1)], lambda k: sems.at[k],
+            )
+        )
+    sums = []
+    for a in range(2):
+        span = pl.ds(2 * a * half, 2 * half)
+        sums.append(total_of(rounds[a], tp2_send[span, :].astype(F32), tp2_recv.at[:, span]))
+    h = h + jnp.concatenate(sums, axis=0)
     part = feed_forward(
         n_kv, h, second_gain[...], w_gate2, w_up2, w_down2, loads[4:7],
         (rs2_send, rs2_recv, act2_own, act2_all),
@@ -512,9 +533,10 @@
     split = q_recv.shape[1] // 2 + 1
     drain("kv", q_recv.at[:, pl.ds(0, split)], send_sems.at[4])
     drain("kv", q_recv.at[:, pl.ds(split, split - 1)], send_sems.at[9])
-    drain("kv", st_recv, o_send_sems.at[0])
-    drain_groups(o_recv, o_send_sems)
-    drain("tp", tp2_recv, send_sems.at[5])
+    for a in range(2):
+        drain("kv", st_recv.at[:, a], o_send_sems.at[a])
+        drain("kv", o_recv.at[:, pl.ds(a * half, half)], o_send_sems.at[2 + a])
+        drain("tp", tp2_recv.at[:, pl.ds(2 * a * half, 2 * half)], send_sems.at[5 * (a + 1)])
     drain("kv", rs2_recv, send_sems.at[6])
     drain("kv", act2_all.at[pl.ds(0, n_kv - 1)], send_sems.at[7])
     total = total_of(copies, fin_send[tp].astype(F32), fin_recv)
@@ -577,9 +599,9 @@
             pltpu.VMEM((pairs, 2 * TILE, 2 * LANES), BF16),
             pltpu.VMEM((pairs, TILE, LANES), BF16),
             pltpu.VMEM((n_kv - 1, pairs, TILE, LANES), BF16),
-            pltpu.VMEM((TILE, 2 * pairs), F32),
-            pltpu.VMEM((n_kv - 1, TILE, 2 * pairs), F32),
-            pltpu.VMEM((4 * pairs, pairs * LANES), BF16),
+            pltpu.VMEM((2, TILE, LANES), BF16),
+            pltpu.VMEM((n_kv - 1, 2, TILE, LANES), BF16),
+            pltpu.VMEM((2 * pairs, pairs // 2 * LANES), BF16),
             pltpu.VMEM((pairs * TILE, LANES), F32),
             *tp_buffers,
             *ffn_buffers,
@@ -588,14 +610,15 @@
             pltpu.SemaphoreType.DMA((6,)),
             pltpu.SemaphoreType.DMA((7 + kv_local * group,)),
             pltpu.SemaphoreType.DMA((8,)),
-            pltpu.SemaphoreType.DMA((10,)),
+            pltpu.SemaphoreType.DMA((11,)),
             pltpu.SemaphoreType.DMA((3,)),
             pltpu.SemaphoreType.DMA((n_kv - 1,)),
             pltpu.SemaphoreType.DMA((n_kv - 1,)),
             pltpu.SemaphoreType.DMA((n_tp - 1,)),
             pltpu.SemaphoreType.DMA((n_tp - 1,)),
-            pltpu.SemaphoreType.DMA((3,)),
-            pltpu.SemaphoreType.DMA((3,)),
+            pltpu.SemaphoreType.DMA((n_tp - 1,)),
+            pltpu.SemaphoreType.DMA((4,)),
+            pltpu.SemaphoreType.DMA((4,)),
         ],
         compiler_params=pltpu.CompilerParams(
             collective_id=1, has_side_effects=True, vmem_limit_bytes=VMEM_LIMIT

time: 62.7 us -> 62.2 us (level)
  no operation moved by 1% of the time
where the time goes in v6:
time: 62.2 us; the launch traced here: 62.1 us
  Pallas kernels  61.5 us (99%)
    pallas_call x1, Pallas kernels, on_device(): pl.pallas_call(functools.partial(layer_kernel, n_kv, n_tp, kv_local, grou...  61.5 us

profile of v6, /device:TPU:1, one launch (start us, length us, event | category | flops | bytes accessed | tf_op | source)
XLA Modules:
  0.0 62.1 jit_solution(13486090756417770680)
XLA Ops:
  0.0 61.5 %shard_map.154 = bf16[32,32]{1,0:T(8,128)(2,1)S(1)} custom-call(bf16[32,32]{1,0:T(8,128)(2,1)} %tokens_any.1, f32[1,256]{1,0:T(1,128)} %bitcast.5, f32[1,256]{1,0:T(1,128)} %bitcast.6, f32[1,256]{1,0:T(1,128)} %bitcast.7, f32[1,4]{1,0:T(1,128)} %bitcast.8, f32[1,64]{1,0:T(1,128)} %bitcast.9, bf16[256,1408]{1,0:T(8,128)(2,1)} %gate1_any.1, ...), custom_call_target="tpu_custom_call" | custom-call | tf_op jit(solution)/shard_map/pallas_call | solution.py:569
  61.5 0.6 copy.18

commit v7 on v6

--- a/solution.py
+++ b/solution.py
@@ -416,6 +416,13 @@
         for weight in (w_gate1, w_up1, w_gate2, w_up2):
             weight[:, hidden:] = jnp.zeros((weight.shape[0], weight.shape[1] - hidden), BF16)
     greet()
+    for load in small:
+        load.wait()
+    tp = lax.axis_index("tp")
+    tok_all[tp] = tokens[...]
+    exchange(
+        "tp", lambda d: tokens, lambda k: tok_all.at[tp], send_sems.at[0], lambda k: once_sems.at[0]
+    )
     cache_loads = start_loads(
         tuple(
             (cache.at[pl.ds((2 * a + i) * half, half)], buf.at[pl.ds(a * half, half), :, lanes])
@@ -424,13 +431,6 @@
             for i, lanes in enumerate((pl.ds(0, LANES), pl.ds(LANES, LANES)))
         ),
         cache_sems,
-    )
-    for load in small:
-        load.wait()
-    tp = lax.axis_index("tp")
-    tok_all[tp] = tokens[...]
-    exchange(
-        "tp", lambda d: tokens, lambda k: tok_all.at[tp], send_sems.at[0], lambda k: once_sems.at[0]
     )
     selector(sel)
     drain("tp", tok_all.at[pl.ds(0, n_tp - 1)], once_sems.at[0])

time: 62.2 us -> 62.2 us (level)
  no operation moved by 1% of the time
where the time goes in v7:
time: 62.2 us; the launch traced here: 62.1 us
  Pallas kernels  61.5 us (99%)
    pallas_call x1, Pallas kernels, on_device(): pl.pallas_call(functools.partial(layer_kernel, n_kv, n_tp, kv_local, grou...  61.5 us

profile of v7, /device:TPU:1, one launch (start us, length us, event | category | flops | bytes accessed | tf_op | source)
XLA Modules:
  0.0 62.1 jit_solution(6915356559848740821)
XLA Ops:
  0.0 61.5 %shard_map.154 = bf16[32,32]{1,0:T(8,128)(2,1)S(1)} custom-call(bf16[32,32]{1,0:T(8,128)(2,1)} %tokens_any.1, f32[1,256]{1,0:T(1,128)} %bitcast.5, f32[1,256]{1,0:T(1,128)} %bitcast.6, f32[1,256]{1,0:T(1,128)} %bitcast.7, f32[1,4]{1,0:T(1,128)} %bitcast.8, f32[1,64]{1,0:T(1,128)} %bitcast.9, bf16[256,1408]{1,0:T(8,128)(2,1)} %gate1_any.1, ...), custom_call_target="tpu_custom_call" | custom-call | tf_op jit(solution)/shard_map/pallas_call | solution.py:569
  61.5 0.6 copy.18
